TPU v7x, 512 devices: a whole 4x8x8 slice. The times are simulated.
512 devices in a mesh: fs: 64 (over z, y), tp: 8 (over x, core).
Axes of the slice: x: 4, y: 8, z: 8, core: 2. Of those that a mesh axis runs over, the one named last changes fastest.
Arguments:
- tokens: bfloat16 [24576, 2048], P('fs', 'tp'), may hold values from -60 to 60
- gain_mixer: float32 [2048], P('tp'), may hold values from 0.1 to 1.9
- w_in: bfloat16 [2048, 1024], P('fs', 'tp'), may hold values from -0.125 to 0.125
- pool_scale: float32 [1024], P('tp'), may hold values from 0.1 to 1.9
- w_pool_out: bfloat16 [2048, 1024], P('fs', 'tp'), may hold values from -0.5 to 0.5
- gain_mid: float32 [2048], P('tp'), may hold values from 0.1 to 1.9
- w_ff1: bfloat16 [2048, 8192], P('fs', 'tp'), may hold values from -0.125 to 0.125
- w_ff2: bfloat16 [2048, 8192], P('fs', 'tp'), may hold values from -0.1875 to 0.1875
- gain_out: float32 [2048], P('tp'), may hold values from 0.1 to 1.9
Outputs:
- layer_out: bfloat16 [24576, 2048], P('fs', 'tp')
All inputs are finite; a program needn't handle non-finite values.
Results may differ from a plain program's by a relative error of at most 0.017.
Values may be sent and summed in bfloat16 or wider, within the bound.
No kernel may reach another device: no remote copies, remote signals or barrier semaphores. Data moves between devices by JAX's collectives and lax.ppermute only.
A program may use at most 64 MiB of HBM per device.

v0:
```python
import jax
import jax.numpy as jnp
from jax import lax
from jax.sharding import PartitionSpec as P

norm_eps = 1e-05
residual_alpha = 2.0**0.25


def from_everyone(array, axis):
    count = lax.axis_size(axis)
    return lax.all_to_all(
        jnp.broadcast_to(array[None], (count, *array.shape)), axis, 0, 0, tiled=True
    )


def of_everyone(array, axis):
    return from_everyone(array, axis).sum(axis=0)


def packed_total(arrays, axis):
    vector, at, gathered = (jnp.concatenate([a.reshape(-1) for a in arrays]), 0, [])
    subtotal = of_everyone(vector, axis)
    for a in arrays:
        gathered.append(subtotal[at : at + a.size].reshape(a.shape))
        at += a.size
    return tuple(gathered)


def joined_along(tiles, dim):
    tiles = jnp.moveaxis(tiles, 0, dim)
    shape = tiles.shape
    return tiles.reshape(*shape[:dim], shape[dim] * shape[dim + 1], *shape[dim + 2 :])


def gathered_copies(array, axis, dim):
    return joined_along(from_everyone(array, axis), dim)


def in_blocks(array, dim, count):
    shape = array.shape
    tiles = array.reshape(*shape[:dim], count, shape[dim] // count, *shape[dim + 1 :])
    return jnp.moveaxis(tiles, dim, 0)


def summed_on_arrival(array, axis, dim):
    tiles = in_blocks(array, dim, lax.axis_size(axis))
    arrived = lax.all_to_all(tiles, axis, split_axis=0, concat_axis=0, tiled=True)
    return arrived.astype(jnp.float32).sum(axis=0)


def row_norm(value, gain):
    width = value.shape[1] * lax.axis_size("tp")
    total, squares = packed_total((jnp.sum(value, axis=1), jnp.sum(value * value, axis=1)), "tp")
    mean = (total / width)[:, None]
    spread = (squares / width)[:, None] - mean * mean
    return (value - mean) * lax.rsqrt(spread + norm_eps) * gain


def shifted(value, steps):
    return jnp.pad(value, ((steps, 0), (0, 0)))[: value.shape[0]]


def project_rows(weight, left):
    return lax.dot_general(
        weight, left, (((1,), (1,)), ((), ())), preferred_element_type=jnp.float32
    )


def fold_features(weight, piece):
    return jnp.dot(piece, weight, preferred_element_type=jnp.float32)


def fold_pooled(weight_cols, channels, total, piece):
    for index in range(piece.shape[1] // channels):
        block = piece[:, index * channels : (index + 1) * channels]
        columns = lax.dynamic_slice_in_dim(weight_cols, index * channels, channels, 1)
        term = lax.dot_general(
            block, columns, (((1,), (1,)), ((), ())), preferred_element_type=jnp.float32
        )
        total = total + term.astype(jnp.bfloat16).astype(jnp.float32)
    return total


def local(tokens, gain_mixer, w_in, pool_scale, w_pool_out, gain_mid, w_ff1, w_ff2, gain_out):
    xf = tokens.astype(jnp.float32)
    length = tokens.shape[0]
    local_width = tokens.shape[1]
    mixed_in = row_norm(xf, gain_mixer).astype(jnp.bfloat16)
    in_full = gathered_copies(w_in, "fs", 0)
    channels = w_in.shape[1]
    pool_in = fold_features(in_full, gathered_copies(mixed_in, "tp", 1))
    uf = pool_in.astype(jnp.bfloat16).astype(jnp.float32)
    group_width = channels * lax.axis_size("tp") // 4
    channel = lax.axis_index("tp") * channels + jnp.arange(channels, dtype=jnp.int32)
    group = channel // group_width
    sum_two = uf + shifted(uf, 1)
    sum_four = sum_two + shifted(sum_two, 2)
    sum_eight = sum_four + shifted(sum_four, 4)
    sum_sixteen = sum_eight + shifted(sum_eight, 8)
    window_sum = jnp.where(
        group == 0,
        sum_two,
        jnp.where(group == 1, sum_four, jnp.where(group == 2, sum_eight, sum_sixteen)),
    )
    window = jnp.where(
        group == 0, 2.0, jnp.where(group == 1, 4.0, jnp.where(group == 2, 8.0, 16.0))
    ).astype(jnp.float32)
    position = jnp.arange(length, dtype=jnp.float32)[:, None]
    count = jnp.minimum(position + 1.0, window[None, :])
    pooled = ((window_sum / count - uf) * pool_scale).astype(jnp.bfloat16)
    out_full = gathered_copies(w_pool_out, "fs", 0)
    weight_cols = lax.all_to_all(out_full, "tp", split_axis=0, concat_axis=1, tiled=True)
    blank = jnp.zeros((length, local_width), jnp.float32)
    mixer_out = fold_pooled(weight_cols, channels, blank, gathered_copies(pooled, "tp", 1)).astype(
        jnp.bfloat16
    )
    middle = row_norm(residual_alpha * xf + mixer_out.astype(jnp.float32), gain_mid).astype(
        jnp.bfloat16
    )
    up_full = lax.all_gather(w_ff1, "fs", axis=0, tiled=True)
    upward = fold_features(up_full, gathered_copies(middle, "tp", 1))
    hidden = jnp.square(jax.nn.relu(upward)).astype(jnp.bfloat16)
    down_full = lax.all_gather(w_ff2, "fs", axis=0, tiled=True)
    ff_out = summed_on_arrival(project_rows(down_full, hidden).astype(jnp.bfloat16), "tp", 0)
    ff_out = ff_out.astype(jnp.bfloat16).T
    result = row_norm(
        residual_alpha * middle.astype(jnp.float32) + ff_out.astype(jnp.float32), gain_out
    )
    return result.astype(jnp.bfloat16)


def solution(mesh):
    return jax.shard_map(
        local,
        mesh=mesh,
        in_specs=(
            P("fs", "tp"),
            P("tp"),
            P("fs", "tp"),
            P("tp"),
            P("fs", "tp"),
            P("tp"),
            P("fs", "tp"),
            P("fs", "tp"),
            P("tp"),
        ),
        out_specs=P("fs", "tp"),
        check_vma=False,
    )
```

profile of v0, /device:TPU:1, one launch (start us, length us, event | category | flops | bytes accessed | tf_op | source)
XLA Modules:
  0.0 242.3 jit_solution(4245685657709784299)
XLA Ops:
  6.5 0.7 all-gather.3.cloned.1.call-update
  7.3 1.1 copy.35
  8.5 13.9 %all_to_all.67 = f32[8,1,768]{2,1,0:T(1,128)S(1)} all-to-all(f32[8,1,768]{2,1,0:T(1,128)S(1)} %broadcast_in_dim.42), channel_id=1, replica_groups=mesh['fs'=64,'tp'=8] {'tp'}, dimensions={0} | all-to-all | bytes 49152 | tf_op jit(solution)/shard_map/all_to_all | solution.py:12
  22.3 0.8 broadcast_in_dim.44
  23.1 29.9 %all_to_all.68 = bf16[64,32,128]{2,1,0:T(8,128)(2,1)S(1)} all-to-all(bf16[64,32,128]{2,1,0:T(8,128)(2,1)S(1)} %broadcast_in_dim.44), channel_id=1, replica_groups=mesh['fs'=64,'tp'=8] {'fs'}, dimensions={0} | all-to-all | bytes 1048576 | tf_op jit(solution)/shard_map/all_to_all | solution.py:12
  53.0 0.9 broadcast_in_dim.96
  54.0 8.3 %all-to-all-start.4 = ((bf16[64,32,128]{2,1,0:T(8,128)(2,1)}), bf16[64,32,128]{2,1,0:T(8,128)(2,1)}, u32[]{:S(2)}, u32[]{:S(2)}) async-start(bf16[64,32,128]{2,1,0:T(8,128)(2,1)} %broadcast_in_dim.96), calls=%async_computation.4 | async-start | bytes 1048576 | tf_op jit(solution)/shard_map/all_to_all | solution.py:12
  62.3 0.7 all-gather.5.cloned.1.call-update
  63.2 15.6 %all-to-all-done.4 = bf16[64,32,128]{2,1,0:T(8,128)(2,1)} async-done(((bf16[64,32,128]{2,1,0:T(8,128)(2,1)}), bf16[64,32,128]{2,1,0:T(8,128)(2,1)}, u32[]{:S(2)}, u32[]{:S(2)}) %all-to-all-start.4) | async-done | bytes 524320 | tf_op jit(solution)/shard_map/all_to_all | solution.py:12
  78.7 1.4 broadcast_in_dim.43
  80.1 7.5 %all-to-all-start.1 = ((bf16[8,384,256]{1,2,0:T(8,128)(2,1)}), bf16[8,384,256]{1,2,0:T(8,128)(2,1)S(1)}, u32[]{:S(2)}, u32[]{:S(2)}) async-start(bf16[8,384,256]{1,2,0:T(8,128)(2,1)} %broadcast_in_dim.43), calls=%async_computation.1 | async-start | bytes 3145728 | tf_op jit(solution)/shard_map/all_to_all | solution.py:12
  87.6 20.6 %all-to-all-done.1 = bf16[8,384,256]{1,2,0:T(8,128)(2,1)S(1)} async-done(((bf16[8,384,256]{1,2,0:T(8,128)(2,1)}), bf16[8,384,256]{1,2,0:T(8,128)(2,1)S(1)}, u32[]{:S(2)}, u32[]{:S(2)}) %all-to-all-start.1) | async-done | bytes 1572896 | tf_op jit(solution)/shard_map/all_to_all | solution.py:12
  108.2 4.4 %all-to-all-start.5 = ((bf16[8,256,128]{2,1,0:T(8,128)(2,1)}), bf16[8,256,128]{2,1,0:T(8,128)(2,1)S(1)}, u32[]{:S(2)}, u32[]{:S(2)}) async-start(bf16[8,256,128]{2,1,0:T(8,128)(2,1)} %bitcast.5), calls=%async_computation.5 | async-start | bytes 1048576 | tf_op jit(solution)/shard_map/all_to_all | solution.py:113
  113.5 8.4 %all-to-all-done.5 = bf16[8,256,128]{2,1,0:T(8,128)(2,1)S(1)} async-done(((bf16[8,256,128]{2,1,0:T(8,128)(2,1)}), bf16[8,256,128]{2,1,0:T(8,128)(2,1)S(1)}, u32[]{:S(2)}, u32[]{:S(2)}) %all-to-all-start.5) | async-done | bytes 524320 | tf_op jit(solution)/shard_map/all_to_all | solution.py:113
  121.9 1.0 broadcast_in_dim.51
  122.9 4.4 %all-to-all-start.3 = ((bf16[8,384,128]{1,2,0:T(8,128)(2,1)}), bf16[8,384,128]{1,2,0:T(8,128)(2,1)S(1)}, u32[]{:S(2)}, u32[]{:S(2)}) async-start(bf16[8,384,128]{1,2,0:T(8,128)(2,1)} %broadcast_in_dim.51), calls=%async_computation.3 | async-start | bytes 1572864 | tf_op jit(solution)/shard_map/all_to_all | solution.py:12
  127.6 12.0 %all-to-all-done.3 = bf16[8,384,128]{1,2,0:T(8,128)(2,1)S(1)} async-done(((bf16[8,384,128]{1,2,0:T(8,128)(2,1)}), bf16[8,384,128]{1,2,0:T(8,128)(2,1)S(1)}, u32[]{:S(2)}, u32[]{:S(2)}) %all-to-all-start.3) | async-done | bytes 786464 | tf_op jit(solution)/shard_map/all_to_all | solution.py:12
  141.7 8.1 %all_to_all.69 = f32[8,1,768]{2,1,0:T(1,128)S(1)} all-to-all(f32[8,1,768]{2,1,0:T(1,128)S(1)} %broadcast_in_dim.97), channel_id=1, replica_groups=mesh['fs'=64,'tp'=8] {'tp'}, dimensions={0} | all-to-all | bytes 49152 | tf_op jit(solution)/shard_map/all_to_all | solution.py:12
  150.1 23.7 %all_to_all.70 = bf16[8,384,256]{1,2,0:T(8,128)(2,1)S(1)} all-to-all(bf16[8,384,256]{1,2,0:T(8,128)(2,1)S(1)} %broadcast_in_dim.98), channel_id=1, replica_groups=mesh['fs'=64,'tp'=8] {'tp'}, dimensions={0} | all-to-all | bytes 3145728 | tf_op jit(solution)/shard_map/all_to_all | solution.py:12
  173.8 15.2 %all-gather.5.cloned.1.call-done = bf16[2048,1024]{1,0:T(8,128)(2,1)} async-done(((bf16[32,1024]{1,0:T(8,128)(2,1)}), bf16[2048,1024]{1,0:T(8,128)(2,1)}) %all-gather.5.cloned.1.call-update) | async-done | bytes 4194320 | tf_op jit(solution)/shard_map/all_gather | solution.py:124
  189.0 6.9 %convolution_convert_fusion = bf16[384,2048]{1,0:T(8,128)(2,1)S(1)} fusion(bf16[2048,1024]{1,0:T(8,128)(2,1)} %all-gather.5.cloned.1.call-done, bf16[384,2048]{0,1:T(8,128)(2,1)S(1)} %bitcast.51, bf16[2048,1024]{1,0:T(8,128)(2,1)} %all-gather.3.cloned.1.call-done), kind=kOutput, calls=%fused_computation | convolution fusion | flops 3223191552 | bytes 11534336 | tf_op jit(solution)/shard_map/dot_general | solution.py:65
  196.0 29.7 %all_to_all.71 = bf16[8,256,384]{1,2,0:T(8,128)(2,1)S(1)} all-to-all(bf16[8,256,384]{1,2,0:T(8,128)(2,1)S(1)} %bitcast.32), channel_id=1, replica_groups=mesh['fs'=64,'tp'=8] {'tp'}, dimensions={0} | all-to-all | bytes 3145728 | tf_op jit(solution)/shard_map/all_to_all | solution.py:48
  226.3 8.1 %all_to_all.72 = f32[8,1,768]{2,1,0:T(1,128)S(1)} all-to-all(f32[8,1,768]{2,1,0:T(1,128)S(1)} %broadcast_in_dim.99), channel_id=1, replica_groups=mesh['fs'=64,'tp'=8] {'tp'}, dimensions={0} | all-to-all | bytes 49152 | tf_op jit(solution)/shard_map/all_to_all | solution.py:12
  234.7 0.8 copy.44
  (53 shorter events, 4.9 us)
Async XLA Ops:
  6.5 46.5 %copy-start.1 = (bf16[32,128]{1,0:T(8,128)(2,1)S(1)}, bf16[32,128]{1,0:T(8,128)(2,1)}, u32[]{:S(2)}) copy-start(bf16[32,128]{1,0:T(8,128)(2,1)} %param.13) | copy-start | bytes 24580
  6.5 167.2 %all-gather.3.cloned.1.call-start = ((), (), s32[]{:S(2)}) async-start(), calls=%async_computation.10 | async-start | bytes 4259840 | tf_op jit(solution)/shard_map/all_gather | solution.py:121
  22.3 40.7 %copy-start.2 = (f32[256]{0:T(256)S(1)}, f32[256]{0:T(256)}, u32[]{:S(2)}) copy-start(f32[256]{0:T(256)} %param.10) | copy-start | bytes 3076
  54.0 24.8 %all-to-all-start.4 = ((bf16[64,32,128]{2,1,0:T(8,128)(2,1)}), bf16[64,32,128]{2,1,0:T(8,128)(2,1)}, u32[]{:S(2)}, u32[]{:S(2)}) async-start(bf16[64,32,128]{2,1,0:T(8,128)(2,1)} %broadcast_in_dim.96), calls=%async_computation.4 | async-start | bytes 1048576 | tf_op jit(solution)/shard_map/all_to_all | solution.py:12
  62.3 126.7 %all-gather.5.cloned.1.call-start = ((), (), s32[]{:S(2)}) async-start(), calls=%async_computation.11 | async-start | bytes 4259840 | tf_op jit(solution)/shard_map/all_gather | solution.py:124
  80.1 28.1 %all-to-all-start.1 = ((bf16[8,384,256]{1,2,0:T(8,128)(2,1)}), bf16[8,384,256]{1,2,0:T(8,128)(2,1)S(1)}, u32[]{:S(2)}, u32[]{:S(2)}) async-start(bf16[8,384,256]{1,2,0:T(8,128)(2,1)} %broadcast_in_dim.43), calls=%async_computation.1 | async-start | bytes 3145728 | tf_op jit(solution)/shard_map/all_to_all | solution.py:12
  108.2 13.7 %all-to-all-start.5 = ((bf16[8,256,128]{2,1,0:T(8,128)(2,1)}), bf16[8,256,128]{2,1,0:T(8,128)(2,1)S(1)}, u32[]{:S(2)}, u32[]{:S(2)}) async-start(bf16[8,256,128]{2,1,0:T(8,128)(2,1)} %bitcast.5), calls=%async_computation.5 | async-start | bytes 1048576 | tf_op jit(solution)/shard_map/all_to_all | solution.py:113
  112.5 0.7 copy-start.4
  122.9 16.6 %all-to-all-start.3 = ((bf16[8,384,128]{1,2,0:T(8,128)(2,1)}), bf16[8,384,128]{1,2,0:T(8,128)(2,1)S(1)}, u32[]{:S(2)}, u32[]{:S(2)}) async-start(bf16[8,384,128]{1,2,0:T(8,128)(2,1)} %broadcast_in_dim.51), calls=%async_computation.3 | async-start | bytes 1572864 | tf_op jit(solution)/shard_map/all_to_all | solution.py:12
  140.9 9.0 %copy-start = (f32[256]{0:T(256)S(1)}, f32[256]{0:T(256)}, u32[]{:S(2)}) copy-start(f32[256]{0:T(256)} %param.14) | copy-start | bytes 3076
  225.7 8.8 %copy-start.3 = (f32[256]{0:T(256)S(1)}, f32[256]{0:T(256)}, u32[]{:S(2)}) copy-start(f32[256]{0:T(256)} %param.17) | copy-start | bytes 3076
Sparse Core Ops, SparseCore 0:
  10.4 92.4 all-gather.2
  106.0 82.9 all-gather.4
where the time goes:
time: 243 us; the launch traced here: 242 us
  blocking collectives  113 us (47%)
  waiting for transfers between devices  73.1 us (30%)
  starting transfers between devices  24.6 us (10%)
  between operations  13.7 us (6%)
  matrix products  9.6 us (4%)
  local copies, waits for them, and re-layouts  6.79 us (3%)
    all_to_all x5, blocking collectives, from_everyone(): lax.all_to_all(jnp.broadcast_to(array[None], (count, *array.shape)), axis...  83.6 us
    all_to_all x3, waiting for transfers between devices, from_everyone(): lax.all_to_all(jnp.broadcast_to(array[None], (count, *array.shape)), axis...  48.1 us
    all_to_all x1, blocking collectives, summed_on_arrival(): lax.all_to_all(tiles, axis, split_axis=0, concat_axis=0, tiled=True)  29.7 us
    all_to_all x3, starting transfers between devices, from_everyone(): lax.all_to_all(jnp.broadcast_to(array[None], (count, *array.shape)), axis...  20.2 us
    all_gather x1, waiting for transfers between devices, local(): down_full = lax.all_gather(w_ff2, 'fs', axis=0, tiled=True)  15.2 us
    all_to_all x1, waiting for transfers between devices, local(): lax.all_to_all(out_full, 'tp', split_axis=0, concat_axis=1, tiled=True)  8.4 us
    dot_general x1, matrix products, project_rows(): lax.dot_general(weight, left, (((1,), (1,)), ((), ())), preferred_element...  6.89 us
  transfers between devices with their start and end apart: 6, of which 5 were waited for; matrix products, arithmetic and copies ran while one was open for 4% of the time, Pallas kernels for 0%

commit v1 on v0

v1 whole, which is shorter than its diff:
```python
import functools

import jax
import jax.numpy as jnp
from jax import lax
from jax.experimental import pallas as pl
from jax.experimental.pallas import tpu as pltpu
from jax.sharding import Mesh, PartitionSpec as P

norm_eps = 1e-05
residual_alpha = 2.0**0.25
FS = ("z", "y")
TP = ("x", "core")
bf16 = jnp.bfloat16
f32 = jnp.float32
VMEM_LIMIT = 60 * 1024 * 1024


def everyone(array, axis):
    count = lax.axis_size(axis)
    return lax.all_to_all(
        jnp.broadcast_to(array[None], (count, *array.shape)), axis, 0, 0, tiled=True
    )


def gather_tp(piece):
    return everyone(everyone(piece, "x"), "core")


def scatter_sum_tp(parts):
    both = lax.all_to_all(parts, "core", 0, 0, tiled=True).astype(f32)
    chip = (both[0] + both[1]).astype(bf16)
    four = lax.all_to_all(chip, "x", 0, 0, tiled=True).astype(f32)
    return (four[0] + four[1]) + (four[2] + four[3])


def row_statistics(load, blocks, width):
    total = None
    for b in range(blocks):
        s = jnp.sum(load(b), axis=1, keepdims=True)
        total = s if total is None else total + s
    mean = total / width
    spread = None
    for b in range(blocks):
        c = load(b) - mean
        s = jnp.sum(c * c, axis=1, keepdims=True)
        spread = s if spread is None else spread + s
    return mean, lax.rsqrt(spread / width + norm_eps)


def shift_down(value, steps, row):
    return jnp.where(row >= steps, pltpu.roll(value, steps, 0), 0.0)


def mixer_kernel(rows, tok_ref, gain_ref, w_in_ref, w_out_ref, scale_ref, out_ref, mixed_ref):
    tiles = 3
    step = rows // tiles
    for t in range(tiles):
        part = pl.ds(t * step, step)
        load = lambda b: tok_ref[b % 2, b // 2, part, :].astype(f32)
        mean, inverse = row_statistics(load, 8, 2048)
        for b in range(8):
            columns = slice(b * 256, (b + 1) * 256)
            mixed = (load(b) - mean) * inverse * gain_ref[:, columns]
            mixed_ref[part, columns] = mixed.astype(bf16)
    pool_in = jnp.dot(mixed_ref[...], w_in_ref[...], preferred_element_type=f32)
    u = pool_in.astype(bf16).astype(f32)
    row = lax.broadcasted_iota(jnp.int32, u.shape, 0)
    group = lax.axis_index("x")
    two = u + shift_down(u, 1, row)
    four = two + shift_down(two, 2, row)
    eight = four + shift_down(four, 4, row)
    sixteen = eight + shift_down(eight, 8, row)
    total = jnp.where(
        group == 0, two, jnp.where(group == 1, four, jnp.where(group == 2, eight, sixteen))
    )
    window = jnp.where(group == 0, 2, jnp.where(group == 1, 4, jnp.where(group == 2, 8, 16)))
    count = jnp.minimum(row + 1, window).astype(f32)
    pooled = ((total / count - u) * scale_ref[...]).astype(bf16)
    for b in range(8):
        rows_out = w_out_ref[b * 256 : (b + 1) * 256, :]
        term = lax.dot_general(
            pooled, rows_out, (((1,), (1,)), ((), ())), preferred_element_type=f32
        )
        out_ref[b % 2, b // 2] = term.astype(bf16)


def ff_kernel(
    rows, tok_ref, mix_ref, gain_ref, w_ref, out_ref, own_ref, mid_ref, hid_ref, w_vmem, sems
):
    pieces = 8
    depth = 2048 // pieces
    copies = []
    for half in range(2):
        for p in range(pieces):
            where = (pl.ds(p * depth, depth), pl.ds(half * 1024, 1024))
            copy = pltpu.make_async_copy(
                w_ref.at[where], w_vmem.at[half, pl.ds(p * depth, depth)], sems.at[half, p]
            )
            copy.start()
            copies.append(copy)
    tiles = 3
    step = rows // tiles
    for t in range(tiles):
        part = pl.ds(t * step, step)
        load = lambda b: residual_alpha * tok_ref[b % 2, b // 2, part, :].astype(f32) + mix_ref[
            b % 2, b // 2, part, :
        ].astype(f32)
        mean, inverse = row_statistics(load, 8, 2048)
        for b in range(8):
            columns = slice(b * 256, (b + 1) * 256)
            mid = (load(b) - mean) * inverse * gain_ref[:, columns]
            mid_ref[b % 2, b // 2, part, :] = mid.astype(bf16)
    own_ref[...] = mid_ref[lax.axis_index("core"), lax.axis_index("x")]
    up = None
    for p in range(pieces):
        copies[p].wait()
        term = jnp.dot(mid_ref[p % 2, p // 2], w_vmem[0, pl.ds(p * depth, depth), :],
                       preferred_element_type=f32)
        up = term if up is None else up + term
    up = jnp.maximum(up, 0.0)
    hid_ref[...] = (up * up).astype(bf16)
    for p in range(pieces):
        copies[pieces + p].wait()
        term = lax.dot_general(
            hid_ref[...],
            w_vmem[1, pl.ds(p * depth, depth), :],
            (((1,), (1,)), ((), ())),
            preferred_element_type=f32,
        )
        out_ref[p % 2, p // 2] = term.astype(bf16)


def vmem(count):
    return [pl.BlockSpec(memory_space=pltpu.VMEM)] * count


def local(tokens, gain_mixer, w_in, pool_scale, w_pool_out, gain_mid, w_ff1, w_ff2, gain_out):
    rows, width = tokens.shape
    channels = w_in.shape[1]
    ff_full = lax.all_gather(jnp.concatenate([w_ff1, w_ff2], axis=1), FS, axis=0, tiled=True)
    small = everyone(jnp.concatenate([w_in, w_pool_out], axis=1), FS).reshape(-1, 2 * channels)
    gains = everyone(jnp.stack([gain_mixer, gain_mid]), TP)
    gains = jnp.moveaxis(gains, 0, 1).reshape(2, 1, 8 * width)
    everything = gather_tp(tokens).reshape(2, 4, rows, width)
    parts = pl.pallas_call(
        functools.partial(mixer_kernel, rows),
        out_shape=jax.ShapeDtypeStruct((2, 4, rows, width), bf16),
        in_specs=vmem(5),
        out_specs=pl.BlockSpec(memory_space=pltpu.VMEM),
        scratch_shapes=[pltpu.VMEM((rows, 8 * width), bf16)],
        compiler_params=pltpu.CompilerParams(vmem_limit_bytes=24 * 1024 * 1024),
        cost_estimate=pl.CostEstimate(flops=4_000_000_000, bytes_accessed=4_000_000, transcendentals=0),
        name="mixer",
    )(everything, gains[0], small[:, :channels], small[:, channels:], pool_scale[None])
    mixer_out = scatter_sum_tp(parts).astype(bf16)
    mixed = gather_tp(mixer_out).reshape(2, 4, rows, width)
    parts, middle = pl.pallas_call(
        functools.partial(ff_kernel, rows),
        out_shape=(
            jax.ShapeDtypeStruct((2, 4, rows, width), bf16),
            jax.ShapeDtypeStruct((rows, width), bf16),
        ),
        in_specs=vmem(3) + [pl.BlockSpec(memory_space=pl.ANY)],
        out_specs=tuple(vmem(2)),
        scratch_shapes=[
            pltpu.VMEM((2, 4, rows, width), bf16),
            pltpu.VMEM((rows, 1024), bf16),
            pltpu.VMEM((2, 2048, 1024), bf16),
            pltpu.SemaphoreType.DMA((2, 8)),
        ],
        compiler_params=pltpu.CompilerParams(vmem_limit_bytes=40 * 1024 * 1024),
        cost_estimate=pl.CostEstimate(flops=8_000_000_000, bytes_accessed=12_000_000, transcendentals=0),
        name="feed_forward",
    )(everything, mixed, gains[1], ff_full)
    ff_out = scatter_sum_tp(parts).astype(bf16)
    value = residual_alpha * middle.astype(f32) + ff_out.astype(f32)
    part_mean = jnp.sum(value, axis=1) / width
    center = value - part_mean[:, None]
    part_spread = jnp.sum(center * center, axis=1)
    packed = jnp.concatenate([part_mean, part_spread])[None]
    means, spreads = jnp.split(everyone(packed, TP)[:, 0], 2, axis=1)
    mean = jnp.mean(means, axis=0)
    away = means - mean
    spread = (jnp.sum(spreads, axis=0) + width * jnp.sum(away * away, axis=0)) / (8 * width)
    result = (value - mean[:, None]) * lax.rsqrt(spread + norm_eps)[:, None] * gain_out
    return result.astype(bf16)


def solution(mesh):
    mesh = Mesh(mesh.devices.reshape(8, 8, 4, 2), FS + TP)
    return jax.shard_map(
        local,
        mesh=mesh,
        in_specs=(
            P(FS, TP),
            P(TP),
            P(FS, TP),
            P(TP),
            P(FS, TP),
            P(TP),
            P(FS, TP),
            P(FS, TP),
            P(TP),
        ),
        out_specs=P(FS, TP),
        check_vma=False,
    )
```

time: 243 us -> 186 us (0.77)
  waiting for transfers between devices: 73.1 us -> 39.3 us
  blocking collectives: 113 us -> 81.2 us
  Pallas kernels: 0 us -> 12.4 us
  matrix products: 9.6 us -> 0 us
  other arithmetic: 1.3 us -> 4.83 us
  local copies, waits for them, and re-layouts: 6.79 us -> 9.52 us
    all_to_all x6 -> x8, blocking collectives: 113 us -> 81.2 us  [the longest x4 42.4 us: everyone(): lax.all_to_all(jnp.broadcast_to(array[None], (count, *array.shape)), axis...]
    all_to_all x4 -> x3, waiting for transfers between devices: 56.5 us -> 39.3 us  [everyone(): lax.all_to_all(jnp.broadcast_to(array[None], (count, *array.shape)), axis...]
    all_gather x2 -> x1, waiting for transfers between devices: 15.2 us -> 0.01 us  [local(): lax.all_gather(jnp.concatenate([w_ff1, w_ff2], axis=1), FS, axis=0, tiled...]
    pallas_call x0 -> x2, Pallas kernels: none -> 12.4 us  [the longest x1 9.6 us: local(): pl.pallas_call(functools.partial(ff_kernel, rows), out_shape=(jax.ShapeDt...]
    dot_general x10 -> x0, matrix products: 9.6 us -> none  [the longest x1 6.89 us: project_rows(): lax.dot_general(weight, left, (((1,), (1,)), ((), ())), preferred_element...]
    unnamed x11 -> x13, local copies, waits for them, and re-layouts: 1.11 us -> 3.58 us
    all_to_all x4 -> x3, starting transfers between devices: 24.5 us -> 24 us  [everyone(): lax.all_to_all(jnp.broadcast_to(array[None], (count, *array.shape)), axis...]
  transfers between devices with their start and end apart: 6 -> 4, of which waited for: 5 -> 3; matrix products, arithmetic and copies ran while one was open for 4% -> 4% of each run, Pallas kernels for 0% -> 2%
where the time goes in v1:
time: 186 us; the launch traced here: 185 us
  blocking collectives  81.2 us (44%)
  waiting for transfers between devices  39.3 us (21%)
  starting transfers between devices  24 us (13%)
  between operations  13.6 us (7%)
  Pallas kernels  12.4 us (7%)
  local copies, waits for them, and re-layouts  9.52 us (5%)
  other arithmetic  4.83 us (3%)
    all_to_all x4, blocking collectives, everyone(): lax.all_to_all(jnp.broadcast_to(array[None], (count, *array.shape)), axis...  42.4 us
    all_to_all x3, waiting for transfers between devices, everyone(): lax.all_to_all(jnp.broadcast_to(array[None], (count, *array.shape)), axis...  39.3 us
    all_to_all x2, blocking collectives, scatter_sum_tp(): four = lax.all_to_all(chip, 'x', 0, 0, tiled=True).astype(f32)  28.8 us
    all_to_all x3, starting transfers between devices, everyone(): lax.all_to_all(jnp.broadcast_to(array[None], (count, *array.shape)), axis...  24 us
    all_to_all x2, blocking collectives, scatter_sum_tp(): both = lax.all_to_all(parts, 'core', 0, 0, tiled=True).astype(f32)  9.99 us
    pallas_call x1, Pallas kernels, local(): pl.pallas_call(functools.partial(ff_kernel, rows), out_shape=(jax.ShapeDt...  9.6 us
    broadcast_in_dim x7, local copies, waits for them, and re-layouts, everyone(): jnp.broadcast_to(array[None], (count, *array.shape))  4.65 us
  transfers between devices with their start and end apart: 4, of which 3 were waited for; matrix products, arithmetic and copies ran while one was open for 4% of the time, Pallas kernels for 2%

profile of v1, /device:TPU:1, one launch (start us, length us, event | category | flops | bytes accessed | tf_op | source)
XLA Modules:
  0.0 184.9 jit_solution(1477677366178525777)
XLA Ops:
  6.5 1.6 pad_maximum_fusion
  8.1 0.7 pad_maximum_fusion.3
  8.8 13.8 %all_to_all.55 = f32[8,2,256]{2,1,0:T(2,128)S(1)} all-to-all(f32[8,2,256]{2,1,0:T(2,128)S(1)} %broadcast_in_dim.20), channel_id=1, replica_groups=mesh['z'=8,'y'=8,'x'=4,'core'=2] {'x','core'}, dimensions={0} | all-to-all | bytes 32768 | tf_op jit(solution)/shard_map/all_to_all | solution.py:21
  22.7 1.9 %broadcast_in_dim.18 = bf16[4,384,256]{2,1,0:T(8,128)(2,1)} broadcast(bf16[384,256]{1,0:T(8,128)(2,1)} %param.9), dimensions={1,2} | broadcast | bytes 983040 | tf_op jit(solution)/shard_map/broadcast_in_dim | solution.py:22
  24.6 3.5 %all-to-all-start = ((bf16[4,384,256]{2,1,0:T(8,128)(2,1)}), bf16[4,384,256]{2,1,0:T(8,128)(2,1)S(1)}, u32[]{:S(2)}, u32[]{:S(2)}) async-start(bf16[4,384,256]{2,1,0:T(8,128)(2,1)} %broadcast_in_dim.18), calls=%async_computation | async-start | bytes 1572864 | tf_op jit(solution)/shard_map/all_to_all | solution.py:21
  28.1 11.6 %all-to-all-done = bf16[4,384,256]{2,1,0:T(8,128)(2,1)S(1)} async-done(((bf16[4,384,256]{2,1,0:T(8,128)(2,1)}), bf16[4,384,256]{2,1,0:T(8,128)(2,1)S(1)}, u32[]{:S(2)}, u32[]{:S(2)}) %all-to-all-start) | async-done | bytes 786464 | tf_op jit(solution)/shard_map/all_to_all | solution.py:21
  39.7 1.2 broadcast_in_dim.21
  40.9 12.7 %all-to-all-start.3 = ((bf16[64,32,256]{2,1,0:T(8,128)(2,1)}), bf16[64,32,256]{2,1,0:T(8,128)(2,1)S(1)}, u32[]{:S(2)}, u32[]{:S(2)}) async-start(bf16[64,32,256]{2,1,0:T(8,128)(2,1)} %broadcast_in_dim.21), calls=%async_computation.3 | async-start | bytes 2097152 | tf_op jit(solution)/shard_map/all_to_all | solution.py:21
  53.6 26.9 %all-to-all-done.3 = bf16[64,32,256]{2,1,0:T(8,128)(2,1)S(1)} async-done(((bf16[64,32,256]{2,1,0:T(8,128)(2,1)}), bf16[64,32,256]{2,1,0:T(8,128)(2,1)S(1)}, u32[]{:S(2)}, u32[]{:S(2)}) %all-to-all-start.3) | async-done | bytes 1048608 | tf_op jit(solution)/shard_map/all_to_all | solution.py:21
  80.5 1.4 broadcast_in_dim.19
  82.1 7.9 %all-to-all-start.1 = ((bf16[2,4,384,256]{3,2,1,0:T(8,128)(2,1)}), bf16[2,4,384,256]{3,2,1,0:T(8,128)(2,1)S(1)}, u32[]{:S(2)}, u32[]{:S(2)}) async-start(bf16[2,4,384,256]{3,2,1,0:T(8,128)(2,1)} %broadcast_in_dim.19), calls=%async_computation.1 | async-start | bytes 3145728 | tf_op jit(solution)/shard_map/all_to_all | solution.py:21
  89.9 1.3 fusion.12
  91.2 0.8 all-to-all-done.1.tok_ref
  92.0 2.8 %mixer.1 = bf16[2,4,384,256]{3,2,1,0:T(8,128)(2,1)S(1)} custom-call(bf16[2,4,384,256]{3,2,1,0:T(8,128)(2,1)S(1)} %all-to-all-done.1.tok_ref, f32[1,2048]{1,0:T(1,128)S(1)} %bitcast.21, bf16[2048,128]{1,0:T(8,128)(2,1)S(1)} %get-tuple-element.14.w_in_ref, bf16[2048,128]{1,0:T(8,128)(2,1)S(1)} %get-tuple-element.13.w_out_ref, f32[1,128]{1,0:T(1,128)S(1)} %bitcast.22), custom_call_target="tpu_custom_call" | custom-call | flops 4000000000 | bytes 4000000 | tf_op jit(solution)/shard_map/mixer/pallas_call | solution.py:146
  94.8 5.0 %all_to_all.56 = bf16[2,4,384,256]{3,2,1,0:T(8,128)(2,1)S(1)} all-to-all(bf16[2,4,384,256]{3,2,1,0:T(8,128)(2,1)S(1)} %mixer.1), channel_id=1, replica_groups=mesh['z'=8,'y'=8,'x'=4,'core'=2] {'core'}, dimensions={0} | all-to-all | bytes 3145728 | tf_op jit(solution)/shard_map/all_to_all | solution.py:31
  100.3 14.4 %all_to_all.57 = bf16[4,384,256]{2,1,0:T(8,128)(2,1)S(1)} all-to-all(bf16[4,384,256]{2,1,0:T(8,128)(2,1)S(1)} %fusion.2), channel_id=1, replica_groups=mesh['z'=8,'y'=8,'x'=4,'core'=2] {'x'}, dimensions={0} | all-to-all | bytes 1572864 | tf_op jit(solution)/shard_map/all_to_all | solution.py:33
  115.0 13.6 %all_to_all.58 = bf16[4,384,256]{2,1,0:T(8,128)(2,1)S(1)} all-to-all(bf16[4,384,256]{2,1,0:T(8,128)(2,1)S(1)} %broadcast_in_dim.24), channel_id=1, replica_groups=mesh['z'=8,'y'=8,'x'=4,'core'=2] {'x'}, dimensions={0} | all-to-all | bytes 1572864 | tf_op jit(solution)/shard_map/all_to_all | solution.py:21
  128.7 6.7 %all_to_all.59.mix_ref = bf16[2,4,384,256]{3,2,1,0:T(8,128)(2,1)S(1)} all-to-all(bf16[2,4,384,256]{3,2,1,0:T(8,128)(2,1)S(1)} %broadcast_in_dim.25), channel_id=1, replica_groups=mesh['z'=8,'y'=8,'x'=4,'core'=2] {'core'}, dimensions={0} | all-to-all | bytes 3145728 | tf_op jit(solution)/shard_map/all_to_all | solution.py:21
  135.4 3.4 %copy-done = bf16[2048,2048]{1,0:T(8,128)(2,1)S(1)} copy-done((bf16[2048,2048]{1,0:T(8,128)(2,1)S(1)}, bf16[2048,2048]{1,0:T(8,128)(2,1)}, u32[]{:S(2)}) %copy-start) | copy-done | bytes 8388632
  138.8 9.6 %feed_forward.1 = (bf16[2,4,384,256]{3,2,1,0:T(8,128)(2,1)S(1)}, bf16[384,256]{1,0:T(8,128)(2,1)S(1)}) custom-call(bf16[2,4,384,256]{3,2,1,0:T(8,128)(2,1)S(1)} %all-to-all-done.1.tok_ref, bf16[2,4,384,256]{3,2,1,0:T(8,128)(2,1)S(1)} %all_to_all.59.mix_ref, f32[1,2048]{1,0:T(1,128)S(1)} %bitcast.20, bf16[2048,2048]{1,0:T(8,128)(2,1)S(1)} %copy-done), custom_call_target="tpu_custom_call" | custom-call | flops 8000000000 | bytes 12000000 | tf_op jit(solution)/shard_map/feed_forward/pallas_call | solution.py:158
  148.4 5.0 %all_to_all.60 = bf16[2,4,384,256]{3,2,1,0:T(8,128)(2,1)S(1)} all-to-all(bf16[2,4,384,256]{3,2,1,0:T(8,128)(2,1)S(1)} %get-tuple-element.8), channel_id=1, replica_groups=mesh['z'=8,'y'=8,'x'=4,'core'=2] {'core'}, dimensions={0} | all-to-all | bytes 3145728 | tf_op jit(solution)/shard_map/all_to_all | solution.py:31
  153.8 14.4 %all_to_all.61 = bf16[4,384,256]{2,1,0:T(8,128)(2,1)S(1)} all-to-all(bf16[4,384,256]{2,1,0:T(8,128)(2,1)S(1)} %fusion.3), channel_id=1, replica_groups=mesh['z'=8,'y'=8,'x'=4,'core'=2] {'x'}, dimensions={0} | all-to-all | bytes 1572864 | tf_op jit(solution)/shard_map/all_to_all | solution.py:33
  168.8 8.3 %all_to_all.62 = f32[8,1,768]{2,1,0:T(1,128)S(1)} all-to-all(f32[8,1,768]{2,1,0:T(1,128)S(1)} %broadcast_in_dim.26), channel_id=1, replica_groups=mesh['z'=8,'y'=8,'x'=4,'core'=2] {'x','core'}, dimensions={0} | all-to-all | bytes 49152 | tf_op jit(solution)/shard_map/all_to_all | solution.py:21
  177.2 0.9 multiply_convert_fusion
  (36 shorter events, 2.1 us)
Async XLA Ops:
  6.5 21.6 %copy-start.4 = (bf16[32,128]{1,0:T(8,128)(2,1)S(1)}, bf16[32,128]{1,0:T(8,128)(2,1)}, u32[]{:S(2)}) copy-start(bf16[32,128]{1,0:T(8,128)(2,1)} %param.11) | copy-start | bytes 24580
  6.5 21.6 %copy-start.3 = (bf16[32,128]{1,0:T(8,128)(2,1)S(1)}, bf16[32,128]{1,0:T(8,128)(2,1)}, u32[]{:S(2)}) copy-start(bf16[32,128]{1,0:T(8,128)(2,1)} %param.13) | copy-start | bytes 24580
  6.5 128.8 %all-gather.2.cloned.1.call-start = ((), (), s32[]{:S(2)}) async-start(), calls=%async_computation.11 | async-start | bytes 8519680 | tf_op jit(solution)/shard_map/all_gather | solution.py:141
  24.6 15.1 %all-to-all-start = ((bf16[4,384,256]{2,1,0:T(8,128)(2,1)}), bf16[4,384,256]{2,1,0:T(8,128)(2,1)S(1)}, u32[]{:S(2)}, u32[]{:S(2)}) async-start(bf16[4,384,256]{2,1,0:T(8,128)(2,1)} %broadcast_in_dim.18), calls=%async_computation | async-start | bytes 1572864 | tf_op jit(solution)/shard_map/all_to_all | solution.py:21
  40.9 39.6 %all-to-all-start.3 = ((bf16[64,32,256]{2,1,0:T(8,128)(2,1)}), bf16[64,32,256]{2,1,0:T(8,128)(2,1)S(1)}, u32[]{:S(2)}, u32[]{:S(2)}) async-start(bf16[64,32,256]{2,1,0:T(8,128)(2,1)} %broadcast_in_dim.21), calls=%async_computation.3 | async-start | bytes 2097152 | tf_op jit(solution)/shard_map/all_to_all | solution.py:21
  80.5 1.6 copy-start.2
  82.1 10.0 %all-to-all-start.1 = ((bf16[2,4,384,256]{3,2,1,0:T(8,128)(2,1)}), bf16[2,4,384,256]{3,2,1,0:T(8,128)(2,1)S(1)}, u32[]{:S(2)}, u32[]{:S(2)}) async-start(bf16[2,4,384,256]{3,2,1,0:T(8,128)(2,1)} %broadcast_in_dim.19), calls=%async_computation.1 | async-start | bytes 3145728 | tf_op jit(solution)/shard_map/all_to_all | solution.py:21
  89.9 2.1 %copy-start.1 = (f32[128]{0:T(128)S(1)}, f32[128]{0:T(128)}, u32[]{:S(2)}) copy-start(f32[128]{0:T(128)} %param.12) | copy-start | bytes 1540
  135.4 3.4 %copy-start = (bf16[2048,2048]{1,0:T(8,128)(2,1)S(1)}, bf16[2048,2048]{1,0:T(8,128)(2,1)}, u32[]{:S(2)}) copy-start(bf16[2048,2048]{1,0:T(8,128)(2,1)} %all-gather.2.cloned.1.call-done.w_ref) | copy-start | bytes 25165828
  168.4 8.8 %copy-start.5 = (f32[256]{0:T(256)S(1)}, f32[256]{0:T(256)}, u32[]{:S(2)}) copy-start(f32[256]{0:T(256)} %param.17) | copy-start | bytes 3076
Sparse Core Ops, SparseCore 0:
  10.4 118.1 all-gather.1

commit v2 on v1

v2 whole, which is shorter than its diff:
```python
import functools

import jax
import jax.numpy as jnp
from jax import lax
from jax.experimental import pallas as pl
from jax.experimental.pallas import tpu as pltpu
from jax.sharding import Mesh, PartitionSpec as P


norm_eps = 1e-05
residual_alpha = 2.0**0.25
FS = ("z", "y")
TP = ("x", "core")
EVERY = FS + TP
bf16 = jnp.bfloat16
f32 = jnp.float32
OFFSETS = (0, 1, -1, 2, -2, 3, -3, 4)
MEBI = 1024 * 1024


def device(z, y, x, core):
    return (((z % 8) * 8 + y % 8) * 4 + x % 4) * 2 + core % 2


PLACES = [(z, y, x) for z in range(8) for y in range(8) for x in range(4)]
FIRST = [[device(z, y, x, 0) for z in range(8)] for y in range(8) for x in range(4)] + [
    [device(z, y, x, 1) for y in range(8)] for z in range(8) for x in range(4)
]
SECOND = [[device(z, y, x, 0) for y in range(8)] for z in range(8) for x in range(4)] + [
    [device(z, y, x, 1) for z in range(8)] for y in range(8) for x in range(4)
]


def around(steps):
    return [
        pair
        for z, y, x in PLACES
        for pair in (
            (device(z, y, x, 0), device(z, y + steps, x, 0)),
            (device(z, y, x, 1), device(z + steps, y, x, 1)),
        )
    ]


def along_x(array, steps):
    pairs = [
        (device(z, y, x, c), device(z, y, x + steps, c)) for z, y, x in PLACES for c in range(2)
    ]
    return lax.ppermute(array, EVERY, pairs)


def from_other_core(array):
    return lax.ppermute(array, "core", [(0, 1), (1, 0)])


def everyone(array, axis):
    count = lax.axis_size(axis)
    return lax.all_to_all(
        jnp.broadcast_to(array[None], (count, *array.shape)), axis, 0, 0, tiled=True
    )


def among(array, groups):
    return lax.all_to_all(
        jnp.broadcast_to(array[None], (8, *array.shape)),
        EVERY,
        0,
        0,
        axis_index_groups=groups,
        tiled=True,
    )


def scatter_sum_tp(keep, send):
    chip = (keep.astype(f32) + from_other_core(send).astype(f32)).astype(bf16)
    four = lax.all_to_all(chip, "x", 0, 0, tiled=True).astype(f32)
    return (four[0] + four[1]) + (four[2] + four[3])


def in_three(gain):
    rest, rows = gain, []
    for _ in range(3):
        rows.append(lax.reduce_precision(rest, 8, 7))
        rest = rest - rows[-1]
    return jnp.stack(rows).astype(bf16)


def gain_of(tok_ref, block, rows, first):
    parts = tok_ref[block, pl.ds(rows, 16), :].astype(f32)
    return parts[first : first + 1] + parts[first + 1 : first + 2] + parts[first + 2 : first + 3]


def columns_of(x, core):
    return pl.ds(pl.multiple_of((2 * x + core) * 256, 256), 256)


def row_at(core, source, j):
    at = jnp.where(core == 0, j * 256 + source * 32, source * 256 + j * 32)
    return pl.ds(pl.multiple_of(at, 32), 32)


def row_statistics(loads, width):
    total = None
    for load in loads:
        s = jnp.sum(load(), axis=1, keepdims=True)
        total = s if total is None else total + s
    mean = total / width
    spread = None
    for load in loads:
        c = load() - mean
        s = jnp.sum(c * c, axis=1, keepdims=True)
        spread = s if spread is None else spread + s
    return mean, lax.rsqrt(spread / width + norm_eps)


def shift_down(value, steps, row):
    return jnp.where(row >= steps, pltpu.roll(value, steps, 0), 0.0)


def mixer_kernel(rows, mine_ref, other_ref, small_ref, scale_ref, keep_ref, send_ref, mixed_ref, w_ref):
    x, core = lax.axis_index("x"), lax.axis_index("core")
    for s in range(8):
        for j in range(8):
            w_ref[row_at(core, s, j), :] = small_ref[s, j]
    step = rows // 3
    for t in range(3):
        part = pl.ds(t * step, step)
        blocks = [(ref, r) for ref in (mine_ref, other_ref) for r in range(4)]
        loads = [lambda ref=ref, r=r: ref[r, part, :].astype(f32) for ref, r in blocks]
        mean, inverse = row_statistics(loads, 2048)
        for (ref, r), load in zip(blocks, loads):
            where = columns_of(lax.rem(x + (4 - r), 4), core if ref is mine_ref else 1 - core)
            mixed = (load() - mean) * inverse * gain_of(ref, r, rows, 0)
            mixed_ref[part, where] = mixed.astype(bf16)
    pool_in = jnp.dot(mixed_ref[...], w_ref[:, :128], preferred_element_type=f32)
    u = pool_in.astype(bf16).astype(f32)
    row = lax.broadcasted_iota(jnp.int32, u.shape, 0)
    two = u + shift_down(u, 1, row)
    four = two + shift_down(two, 2, row)
    eight = four + shift_down(four, 4, row)
    sixteen = eight + shift_down(eight, 8, row)
    total = jnp.where(x == 0, two, jnp.where(x == 1, four, jnp.where(x == 2, eight, sixteen)))
    window = jnp.where(x == 0, 2, jnp.where(x == 1, 4, jnp.where(x == 2, 8, 16)))
    count = jnp.minimum(row + 1, window).astype(f32)
    pooled = ((total / count - u) * scale_ref[...]).astype(bf16)
    for xb in range(4):
        for ref, c in ((keep_ref, core), (send_ref, 1 - core)):
            term = lax.dot_general(
                pooled,
                w_ref[columns_of(xb, c), 128:],
                (((1,), (1,)), ((), ())),
                preferred_element_type=f32,
            )
            ref[xb] = term.astype(bf16)


def ff_kernel(rows, mine_ref, other_ref, mix_ref, mix_other_ref, *refs):
    chunks, (keep_ref, send_ref, own_ref, mid_ref, hid_ref, w_ref, sems) = refs[:8], refs[8:]
    x, core = lax.axis_index("x"), lax.axis_index("core")
    place = jnp.where(core == 0, lax.axis_index("y"), lax.axis_index("z"))
    copies = []
    for k, (chunk, offset) in enumerate(zip(chunks, OFFSETS)):
        source = lax.rem(place + (8 - offset), 8)
        for j in range(8):
            copy = pltpu.make_async_copy(
                chunk.at[j], w_ref.at[row_at(core, source, j)], sems.at[k, j]
            )
            copy.start()
            copies.append(copy)
    step = rows // 3
    for t in range(3):
        part = pl.ds(t * step, step)
        blocks = [
            (tok, mix, c, xb)
            for tok, mix, c in ((mine_ref, mix_ref, core), (other_ref, mix_other_ref, 1 - core))
            for xb in range(4)
        ]

        def total(tok, mix, xb):
            r = lax.rem(x + (4 - xb), 4)
            return residual_alpha * tok[r, part, :].astype(f32) + mix[xb, part, :].astype(f32)

        loads = [functools.partial(total, tok, mix, xb) for tok, mix, _, xb in blocks]
        mean, inverse = row_statistics(loads, 2048)
        for (tok, mix, c, xb), load in zip(blocks, loads):
            gain = gain_of(tok, lax.rem(x + (4 - xb), 4), rows, 3)
            mid_ref[part, columns_of(xb, c)] = ((load() - mean) * inverse * gain).astype(bf16)
    own_ref[...] = mid_ref[:, columns_of(x, core)]
    for copy in copies:
        copy.wait()
    for n in range(4):
        where = slice(n * 256, (n + 1) * 256)
        up = jnp.dot(mid_ref[...], w_ref[:, where], preferred_element_type=f32)
        up = jnp.maximum(up, 0.0)
        hid_ref[:, where] = (up * up).astype(bf16)
    for xb in range(4):
        for ref, c in ((keep_ref, core), (send_ref, 1 - core)):
            term = lax.dot_general(
                hid_ref[...],
                w_ref[columns_of(xb, c), 1024:],
                (((1,), (1,)), ((), ())),
                preferred_element_type=f32,
            )
            ref[xb] = term.astype(bf16)


def vmem(count):
    return [pl.BlockSpec(memory_space=pltpu.VMEM)] * count


def mixer(mine, other, small, scale, rows, width, channels):
    block = jax.ShapeDtypeStruct((4, rows, width), bf16)
    return pl.pallas_call(
        functools.partial(mixer_kernel, rows),
        out_shape=(block, block),
        in_specs=vmem(4),
        out_specs=tuple(vmem(2)),
        scratch_shapes=[
            pltpu.VMEM((rows, 8 * width), bf16),
            pltpu.VMEM((8 * width, 2 * channels), bf16),
        ],
        compiler_params=pltpu.CompilerParams(vmem_limit_bytes=24 * MEBI),
        cost_estimate=pl.CostEstimate(flops=4_000_000_000, bytes_accessed=4_000_000, transcendentals=0),
        name="mixer",
    )(mine, other, small, scale)


def feed_forward(mine, other, mix, mix_other, chunks, rows, width):
    block = jax.ShapeDtypeStruct((4, rows, width), bf16)
    return pl.pallas_call(
        functools.partial(ff_kernel, rows),
        out_shape=(block, block, jax.ShapeDtypeStruct((rows, width), bf16)),
        in_specs=vmem(4) + [pl.BlockSpec(memory_space=pl.ANY)] * 8,
        out_specs=tuple(vmem(3)),
        scratch_shapes=[
            pltpu.VMEM((rows, 8 * width), bf16),
            pltpu.VMEM((rows, 1024), bf16),
            pltpu.VMEM((2048, 2048), bf16),
            pltpu.SemaphoreType.DMA((8, 8)),
        ],
        compiler_params=pltpu.CompilerParams(vmem_limit_bytes=30 * MEBI),
        cost_estimate=pl.CostEstimate(flops=8_000_000_000, bytes_accessed=12_000_000, transcendentals=0),
        name="feed_forward",
    )(mine, other, mix, mix_other, *chunks)


def layer(tokens, gain_mixer, w_in, pool_scale, w_pool_out, gain_mid, w_ff1, w_ff2, gain_out):
    rows, width = tokens.shape
    channels = w_in.shape[1]
    packed = jnp.concatenate([w_ff1, w_ff2, w_in, w_pool_out], axis=1)
    first = among(packed, FIRST)
    small = among(first[:, :, 2048:].reshape(256, 2 * channels), SECOND)
    small = small.reshape(8, 8, 32, 2 * channels)
    chunk = first[:, :, :2048]
    chunks = [chunk]
    up, down = chunk, chunk
    for hop in range(4):
        up = lax.ppermute(up, EVERY, around(1))
        chunks.append(up)
        if hop < 3:
            down = lax.ppermute(down, EVERY, around(-1))
            chunks.append(down)
    extended = jnp.concatenate(
        [tokens, in_three(gain_mixer), in_three(gain_mid), jnp.zeros((10, width), bf16)]
    )
    pieces = [extended]
    for steps in (1, 2, 3):
        pieces.append(along_x(extended, steps))
    mine = jnp.stack(pieces)
    other = from_other_core(mine)
    keep, send = mixer(mine, other, small, pool_scale[None], rows, width, channels)
    mixer_out = scatter_sum_tp(keep, send).astype(bf16)
    mix = everyone(mixer_out, "x")
    mix_other = from_other_core(mix)
    keep, send, middle = feed_forward(mine, other, mix, mix_other, chunks, rows, width)
    ff_out = scatter_sum_tp(keep, send).astype(bf16)
    value = residual_alpha * middle.astype(f32) + ff_out.astype(f32)
    part_mean = jnp.sum(value, axis=1) / width
    center = value - part_mean[:, None]
    part_spread = jnp.sum(center * center, axis=1)
    sums = jnp.concatenate([part_mean, part_spread])[None]
    means, spreads = jnp.split(everyone(sums, TP)[:, 0], 2, axis=1)
    mean = jnp.mean(means, axis=0)
    away = means - mean
    spread = (jnp.sum(spreads, axis=0) + width * jnp.sum(away * away, axis=0)) / (8 * width)
    result = (value - mean[:, None]) * lax.rsqrt(spread + norm_eps)[:, None] * gain_out
    return result.astype(bf16)


def solution(mesh):
    mesh = Mesh(mesh.devices.reshape(8, 8, 4, 2), EVERY)
    return jax.shard_map(
        layer,
        mesh=mesh,
        in_specs=(
            P(FS, TP),
            P(TP),
            P(FS, TP),
            P(TP),
            P(FS, TP),
            P(TP),
            P(FS, TP),
            P(FS, TP),
            P(TP),
        ),
        out_specs=P(FS, TP),
        check_vma=False,
    )
```

time: 186 us -> 176 us (0.946)
  starting transfers between devices: 24 us -> 65.5 us
  blocking collectives: 81.2 us -> 49.6 us
  between operations: 13.6 us -> 0.39 us
  waiting for transfers between devices: 39.3 us -> 34.1 us
    ppermute x0 -> x14, starting transfers between devices: none -> 48.8 us  [the longest x4 16.2 us: from_other_core(): return lax.ppermute(array, 'core', [(0, 1), (1, 0)])]
    all_to_all x3 -> x1, waiting for transfers between devices: 39.3 us -> 0.01 us  [everyone(): lax.all_to_all(jnp.broadcast_to(array[None], (count, *array.shape)), axis...]
    ppermute x0 -> x14, waiting for transfers between devices: none -> 34.1 us  [the longest x4 15.6 us: layer(): up = lax.ppermute(up, EVERY, around(1))]
    all_to_all x4 -> x1, blocking collectives: 42.4 us -> 8.4 us  [everyone(): lax.all_to_all(jnp.broadcast_to(array[None], (count, *array.shape)), axis...]
    all_to_all x3 -> x1, starting transfers between devices: 24 us -> 3.49 us  [everyone(): lax.all_to_all(jnp.broadcast_to(array[None], (count, *array.shape)), axis...]
    all_to_all x2 -> x1, blocking collectives: 9.99 us -> 26.9 us  [among(): lax.all_to_all(jnp.broadcast_to(array[None], (8, *array.shape)), EVERY, 0...]
    all_to_all x2 -> x1, blocking collectives: 28.8 us -> 14.3 us  [scatter_sum_tp(): four = lax.all_to_all(chip, 'x', 0, 0, tiled=True).astype(f32)]
    all_to_all x0 -> x2, starting transfers between devices: none -> 13.2 us  [the longest x1 9.74 us: among(): lax.all_to_all(jnp.broadcast_to(array[None], (8, *array.shape)), EVERY, 0...]
  transfers between devices with their start and end apart: 4 -> 17, of which waited for: 3 -> 10; matrix products, arithmetic and copies ran while one was open for 4% -> 2% of each run, Pallas kernels for 2% -> 2%
where the time goes in v2:
time: 176 us; the launch traced here: 175 us
  starting transfers between devices  65.5 us (37%)
  blocking collectives  49.6 us (28%)
  waiting for transfers between devices  34.1 us (19%)
  Pallas kernels  13.7 us (8%)
  local copies, waits for them, and re-layouts  7.99 us (5%)
  other arithmetic  4 us (2%)
    all_to_all x1, blocking collectives, among(): lax.all_to_all(jnp.broadcast_to(array[None], (8, *array.shape)), EVERY, 0...  26.9 us
    ppermute x4, starting transfers between devices, from_other_core(): return lax.ppermute(array, 'core', [(0, 1), (1, 0)])  16.2 us
    ppermute x4, waiting for transfers between devices, layer(): up = lax.ppermute(up, EVERY, around(1))  15.6 us
    all_to_all x1, blocking collectives, scatter_sum_tp(): four = lax.all_to_all(chip, 'x', 0, 0, tiled=True).astype(f32)  14.3 us
    ppermute x3, starting transfers between devices, layer(): down = lax.ppermute(down, EVERY, around(-1))  13.9 us
    pallas_call x1, Pallas kernels, feed_forward(): pl.pallas_call(functools.partial(ff_kernel, rows), out_shape=(block, bloc...  10.1 us
    all_to_all x1, starting transfers between devices, among(): lax.all_to_all(jnp.broadcast_to(array[None], (8, *array.shape)), EVERY, 0...  9.74 us
    ppermute x3, starting transfers between devices, along_x(): return lax.ppermute(array, EVERY, pairs)  9.33 us
  transfers between devices with their start and end apart: 17, of which 10 were waited for; matrix products, arithmetic and copies ran while one was open for 2% of the time, Pallas kernels for 2%

profile of v2, /device:TPU:1, one launch (start us, length us, event | category | flops | bytes accessed | tf_op | source)
XLA Modules:
  0.0 175.3 jit_solution(14325363516717833876)
XLA Ops:
  1.0 26.9 %all_to_all.30 = bf16[8,32,2304]{2,1,0:T(8,128)(2,1)S(1)} all-to-all(bf16[8,32,2304]{2,1,0:T(8,128)(2,1)S(1)} %broadcast_in_dim.17), channel_id=1, replica_groups={{0,64,128,192,256,320,384,448},{2,66,130,194,258,322,386,450},{4,68,132..., dimensions={0} | all-to-all | bytes 2359296 | tf_op jit(solution)/shard_map/all_to_all | solution.py:65
  30.0 9.7 %all-to-all-start.1 = ((bf16[8,256,256]{2,1,0:T(8,128)(2,1)}), bf16[8,256,256]{2,1,0:T(8,128)(2,1)S(1)}, u32[]{:S(2)}, u32[]{:S(2)}) async-start(bf16[8,256,256]{2,1,0:T(8,128)(2,1)} %broadcast_in_dim.19), calls=%async_computation.1 | async-start | bytes 2097152 | tf_op jit(solution)/shard_map/all_to_all | solution.py:65
  40.2 4.4 %collective-permute-start.2 = (bf16[400,256]{1,0:T(8,128)(2,1)S(1)}, bf16[400,256]{1,0:T(8,128)(2,1)S(1)}, u32[]{:S(2)}, u32[]{:S(2)}) collective-permute-start(bf16[400,256]{1,0:T(8,128)(2,1)S(1)} %concatenate.10), channel_id=1, source_target_pairs={{0,6},{1,7},{2,0},{3,1},{4,2},{5,3},{6,4},{7,5},{8,14},{9,15},{10,... | collective-permute-start | bytes 614408 | tf_op jit(solution)/shard_map/ppermute | solution.py:50
  49.5 3.3 %collective-permute-done.1 = bf16[400,256]{1,0:T(8,128)(2,1)S(1)} collective-permute-done((bf16[400,256]{1,0:T(8,128)(2,1)S(1)}, bf16[400,256]{1,0:T(8,128)(2,1)S(1)}, u32[]{:S(2)}, u32[]{:S(2)}) %collective-permute-start.1) | collective-permute-done | bytes 204832 | tf_op jit(solution)/shard_map/ppermute | solution.py:50
  52.8 4.4 %collective-permute-done = bf16[400,256]{1,0:T(8,128)(2,1)S(1)} collective-permute-done((bf16[400,256]{1,0:T(8,128)(2,1)S(1)}, bf16[400,256]{1,0:T(8,128)(2,1)S(1)}, u32[]{:S(2)}, u32[]{:S(2)}) %collective-permute-start) | collective-permute-done | bytes 204832 | tf_op jit(solution)/shard_map/ppermute | solution.py:50
  57.4 4.4 %collective-permute-start.3 = (bf16[4,400,256]{2,1,0:T(8,128)(2,1)S(1)}, bf16[4,400,256]{2,1,0:T(8,128)(2,1)S(1)}, u32[]{:S(2)}, u32[]{:S(2)}) collective-permute-start(bf16[4,400,256]{2,1,0:T(8,128)(2,1)S(1)} %pad_maximum_fusion.mine_ref), channel_id=1, source_target_pairs={{0,1},{1,0},{2,3},{3,2},{4,5},{5,4},{6,7},{7,6},{8,9},{9,8},{10,11... | collective-permute-start | bytes 2457608 | tf_op jit(solution)/shard_map/ppermute | solution.py:54
  63.1 3.4 %collective-permute-start.6 = (bf16[8,32,2048]{2,1,0:T(8,128)(2,1)S(1)}, bf16[8,32,2048]{2,1,0:T(8,128)(2,1)}, u32[]{:S(2)}, u32[]{:S(2)}) collective-permute-start(bf16[8,32,2048]{2,1,0:T(8,128)(2,1)S(1)} %slice.45.refs_0_), channel_id=1, source_target_pairs={{0,8},{1,65},{2,10},{3,67},{4,12},{5,69},{6,14},{7,71},{8,16},{9,7... | collective-permute-start | bytes 3145736 | tf_op jit(solution)/shard_map/ppermute | solution.py:259
  68.6 3.6 %mixer.1 = (bf16[4,384,256]{2,1,0:T(8,128)(2,1)S(1)}, bf16[4,384,256]{2,1,0:T(8,128)(2,1)S(1)}) custom-call(bf16[4,400,256]{2,1,0:T(8,128)(2,1)S(1)} %pad_maximum_fusion.mine_ref, bf16[4,400,256]{2,1,0:T(8,128)(2,1)S(1)} %copy-done.1, bf16[8,8,32,256]{3,2,1,0:T(8,128)(2,1)S(1)} %bitcast.16, f32[1,128]{1,0:T(1,128)S(1)} %bitcast.17), custom_call_target="tpu_custom_call" | custom-call | flops 4000000000 | bytes 4000000 | tf_op jit(solution)/shard_map/mixer/pallas_call | solution.py:214
  74.2 3.7 %collective-permute-start.7 = (bf16[8,32,2048]{2,1,0:T(8,128)(2,1)S(1)}, bf16[8,32,2048]{2,1,0:T(8,128)(2,1)}, u32[]{:S(2)}, u32[]{:S(2)}) collective-permute-start(bf16[8,32,2048]{2,1,0:T(8,128)(2,1)S(1)} %slice.45.refs_0_), channel_id=1, source_target_pairs={{0,56},{1,449},{2,58},{3,451},{4,60},{5,453},{6,62},{7,455},{8,0},... | collective-permute-start | bytes 3145736 | tf_op jit(solution)/shard_map/ppermute | solution.py:262
  83.6 3.5 %all-to-all-start.2 = ((bf16[4,384,256]{2,1,0:T(8,128)(2,1)}), bf16[4,384,256]{2,1,0:T(8,128)(2,1)S(1)}, u32[]{:S(2)}, u32[]{:S(2)}) async-start(bf16[4,384,256]{2,1,0:T(8,128)(2,1)} %add_convert_fusion.1), calls=%async_computation.2 | async-start | bytes 1572864 | tf_op jit(solution)/shard_map/all_to_all | solution.py:77
  87.1 3.1 %collective-permute-done.7.refs_2_ = bf16[8,32,2048]{2,1,0:T(8,128)(2,1)} collective-permute-done((bf16[8,32,2048]{2,1,0:T(8,128)(2,1)S(1)}, bf16[8,32,2048]{2,1,0:T(8,128)(2,1)}, u32[]{:S(2)}, u32[]{:S(2)}) %collective-permute-start.7) | collective-permute-done | bytes 1048608 | tf_op jit(solution)/shard_map/ppermute | solution.py:262
  90.1 4.9 %collective-permute-start.9 = (bf16[8,32,2048]{2,1,0:T(8,128)(2,1)}, bf16[8,32,2048]{2,1,0:T(8,128)(2,1)}, u32[]{:S(2)}, u32[]{:S(2)}) collective-permute-start(bf16[8,32,2048]{2,1,0:T(8,128)(2,1)} %collective-permute-done.7.refs_2_), channel_id=1, source_target_pairs={{0,56},{1,449},{2,58},{3,451},{4,60},{5,453},{6,62},{7,455},{8,0},... | collective-permute-start | bytes 3145736 | tf_op jit(solution)/shard_map/ppermute | solution.py:262
  95.0 2.6 %collective-permute-done.8.refs_3_ = bf16[8,32,2048]{2,1,0:T(8,128)(2,1)} collective-permute-done((bf16[8,32,2048]{2,1,0:T(8,128)(2,1)}, bf16[8,32,2048]{2,1,0:T(8,128)(2,1)}, u32[]{:S(2)}, u32[]{:S(2)}) %collective-permute-start.8) | collective-permute-done | bytes 1048608 | tf_op jit(solution)/shard_map/ppermute | solution.py:259
  100.8 3.5 %all-to-all-start.3 = ((bf16[4,384,256]{2,1,0:T(8,128)(2,1)}), bf16[4,384,256]{2,1,0:T(8,128)(2,1)S(1)}, u32[]{:S(2)}, u32[]{:S(2)}) async-start(bf16[4,384,256]{2,1,0:T(8,128)(2,1)} %broadcast_in_dim.43), calls=%async_computation.3 | async-start | bytes 1572864 | tf_op jit(solution)/shard_map/all_to_all | solution.py:59
  104.3 2.8 %collective-permute-done.9.refs_4_ = bf16[8,32,2048]{2,1,0:T(8,128)(2,1)} collective-permute-done((bf16[8,32,2048]{2,1,0:T(8,128)(2,1)}, bf16[8,32,2048]{2,1,0:T(8,128)(2,1)}, u32[]{:S(2)}, u32[]{:S(2)}) %collective-permute-start.9) | collective-permute-done | bytes 1048608 | tf_op jit(solution)/shard_map/ppermute | solution.py:262
  107.1 5.3 %collective-permute-start.11 = (bf16[8,32,2048]{2,1,0:T(8,128)(2,1)}, bf16[8,32,2048]{2,1,0:T(8,128)(2,1)}, u32[]{:S(2)}, u32[]{:S(2)}) collective-permute-start(bf16[8,32,2048]{2,1,0:T(8,128)(2,1)} %collective-permute-done.9.refs_4_), channel_id=1, source_target_pairs={{0,56},{1,449},{2,58},{3,451},{4,60},{5,453},{6,62},{7,455},{8,0},... | collective-permute-start | bytes 3145736 | tf_op jit(solution)/shard_map/ppermute | solution.py:262
  112.4 2.6 %collective-permute-done.10.refs_5_ = bf16[8,32,2048]{2,1,0:T(8,128)(2,1)} collective-permute-done((bf16[8,32,2048]{2,1,0:T(8,128)(2,1)}, bf16[8,32,2048]{2,1,0:T(8,128)(2,1)}, u32[]{:S(2)}, u32[]{:S(2)}) %collective-permute-start.10) | collective-permute-done | bytes 1048608 | tf_op jit(solution)/shard_map/ppermute | solution.py:259
  116.9 4.5 %collective-permute-start.5 = (bf16[4,384,256]{2,1,0:T(8,128)(2,1)S(1)}, bf16[4,384,256]{2,1,0:T(8,128)(2,1)S(1)}, u32[]{:S(2)}, u32[]{:S(2)}) collective-permute-start(bf16[4,384,256]{2,1,0:T(8,128)(2,1)S(1)} %all-to-all-done.3.mix_ref), channel_id=1, source_target_pairs={{0,1},{1,0},{2,3},{3,2},{4,5},{5,4},{6,7},{7,6},{8,9},{9,8},{10,11... | collective-permute-start | bytes 2359304 | tf_op jit(solution)/shard_map/ppermute | solution.py:54
  121.4 3.0 %collective-permute-done.11.refs_6_ = bf16[8,32,2048]{2,1,0:T(8,128)(2,1)} collective-permute-done((bf16[8,32,2048]{2,1,0:T(8,128)(2,1)}, bf16[8,32,2048]{2,1,0:T(8,128)(2,1)}, u32[]{:S(2)}, u32[]{:S(2)}) %collective-permute-start.11) | collective-permute-done | bytes 1048608 | tf_op jit(solution)/shard_map/ppermute | solution.py:262
  124.4 7.9 %collective-permute-done.12.refs_7_ = bf16[8,32,2048]{2,1,0:T(8,128)(2,1)} collective-permute-done((bf16[8,32,2048]{2,1,0:T(8,128)(2,1)}, bf16[8,32,2048]{2,1,0:T(8,128)(2,1)}, u32[]{:S(2)}, u32[]{:S(2)}) %collective-permute-start.12) | collective-permute-done | bytes 1048608 | tf_op jit(solution)/shard_map/ppermute | solution.py:259
  133.5 10.1 %feed_forward.1 = (bf16[4,384,256]{2,1,0:T(8,128)(2,1)S(1)}, bf16[4,384,256]{2,1,0:T(8,128)(2,1)S(1)}, bf16[384,256]{1,0:T(8,128)(2,1)S(1)}) custom-call(bf16[4,400,256]{2,1,0:T(8,128)(2,1)S(1)} %pad_maximum_fusion.mine_ref, bf16[4,400,256]{2,1,0:T(8,128)(2,1)S(1)} %copy-done.2, bf16[4,384,256]{2,1,0:T(8,128)(2,1)S(1)} %all-to-all-done.3.mix_ref, ...), custom_call_target="tpu_custom_call" | custom-call | flops 8000000000 | bytes 12000000 | tf_op jit(solution)/shard_map/feed_forward/pallas_call | solution.py:231
  143.6 5.3 %collective-permute-start.13 = (bf16[4,384,256]{2,1,0:T(8,128)(2,1)S(1)}, bf16[4,384,256]{2,1,0:T(8,128)(2,1)S(1)}, u32[]{:S(2)}, u32[]{:S(2)}) collective-permute-start(bf16[4,384,256]{2,1,0:T(8,128)(2,1)S(1)} %get-tuple-element.14), channel_id=1, source_target_pairs={{0,1},{1,0},{2,3},{3,2},{4,5},{5,4},{6,7},{7,6},{8,9},{9,8},{10,11... | collective-permute-start | bytes 2359304 | tf_op jit(solution)/shard_map/ppermute | solution.py:54
  151.1 14.3 %all_to_all.31 = bf16[4,384,256]{2,1,0:T(8,128)(2,1)S(1)} all-to-all(bf16[4,384,256]{2,1,0:T(8,128)(2,1)S(1)} %add_convert_fusion), channel_id=1, replica_groups=mesh['z'=8,'y'=8,'x'=4,'core'=2] {'x'}, dimensions={0} | all-to-all | bytes 1572864 | tf_op jit(solution)/shard_map/all_to_all | solution.py:77
  166.0 8.4 %all_to_all.32 = f32[8,1,768]{2,1,0:T(1,128)S(1)} all-to-all(f32[8,1,768]{2,1,0:T(1,128)S(1)} %broadcast_in_dim.44), channel_id=1, replica_groups=mesh['z'=8,'y'=8,'x'=4,'core'=2] {'x','core'}, dimensions={0} | all-to-all | bytes 49152 | tf_op jit(solution)/shard_map/all_to_all | solution.py:59
  (66 shorter events, 29.1 us)
Async XLA Ops:
  29.0 10.8 %copy-start.7 = (f32[256]{0:T(256)S(1)}, f32[256]{0:T(256)}, u32[]{:S(2)}) copy-start(f32[256]{0:T(256)} %param.10) | copy-start | bytes 3076
  29.0 10.8 %copy-start.8 = (f32[256]{0:T(256)S(1)}, f32[256]{0:T(256)}, u32[]{:S(2)}) copy-start(f32[256]{0:T(256)} %param.14) | copy-start | bytes 3076
  29.0 10.9 %copy-start.5 = (bf16[384,256]{1,0:T(8,128)(2,1)S(1)}, bf16[384,256]{1,0:T(8,128)(2,1)}, u32[]{:S(2)}) copy-start(bf16[384,256]{1,0:T(8,128)(2,1)} %param.9) | copy-start | bytes 589828
  30.0 37.4 %all-to-all-start.1 = ((bf16[8,256,256]{2,1,0:T(8,128)(2,1)}), bf16[8,256,256]{2,1,0:T(8,128)(2,1)S(1)}, u32[]{:S(2)}, u32[]{:S(2)}) async-start(bf16[8,256,256]{2,1,0:T(8,128)(2,1)} %broadcast_in_dim.19), calls=%async_computation.1 | async-start | bytes 2097152 | tf_op jit(solution)/shard_map/all_to_all | solution.py:65
  40.2 9.4 %collective-permute-start.2 = (bf16[400,256]{1,0:T(8,128)(2,1)S(1)}, bf16[400,256]{1,0:T(8,128)(2,1)S(1)}, u32[]{:S(2)}, u32[]{:S(2)}) collective-permute-start(bf16[400,256]{1,0:T(8,128)(2,1)S(1)} %concatenate.10), channel_id=1, source_target_pairs={{0,6},{1,7},{2,0},{3,1},{4,2},{5,3},{6,4},{7,5},{8,14},{9,15},{10,... | collective-permute-start | bytes 614408 | tf_op jit(solution)/shard_map/ppermute | solution.py:50
  44.5 8.3 %collective-permute-start.1 = (bf16[400,256]{1,0:T(8,128)(2,1)S(1)}, bf16[400,256]{1,0:T(8,128)(2,1)S(1)}, u32[]{:S(2)}, u32[]{:S(2)}) collective-permute-start(bf16[400,256]{1,0:T(8,128)(2,1)S(1)} %concatenate.10), channel_id=1, source_target_pairs={{0,4},{1,5},{2,6},{3,7},{4,0},{5,1},{6,2},{7,3},{8,12},{9,13},{10,... | collective-permute-start | bytes 614408 | tf_op jit(solution)/shard_map/ppermute | solution.py:50
  47.0 10.3 %collective-permute-start = (bf16[400,256]{1,0:T(8,128)(2,1)S(1)}, bf16[400,256]{1,0:T(8,128)(2,1)S(1)}, u32[]{:S(2)}, u32[]{:S(2)}) collective-permute-start(bf16[400,256]{1,0:T(8,128)(2,1)S(1)} %concatenate.10), channel_id=1, source_target_pairs={{0,2},{1,3},{2,4},{3,5},{4,6},{5,7},{6,0},{7,1},{8,10},{9,11},{10,... | collective-permute-start | bytes 614408 | tf_op jit(solution)/shard_map/ppermute | solution.py:50
  57.3 10.2 %copy-start.3 = (f32[128]{0:T(128)S(1)}, f32[128]{0:T(128)}, u32[]{:S(2)}) copy-start(f32[128]{0:T(128)} %param.12) | copy-start | bytes 1540
  57.4 9.1 %collective-permute-start.3 = (bf16[4,400,256]{2,1,0:T(8,128)(2,1)S(1)}, bf16[4,400,256]{2,1,0:T(8,128)(2,1)S(1)}, u32[]{:S(2)}, u32[]{:S(2)}) collective-permute-start(bf16[4,400,256]{2,1,0:T(8,128)(2,1)S(1)} %pad_maximum_fusion.mine_ref), channel_id=1, source_target_pairs={{0,1},{1,0},{2,3},{3,2},{4,5},{5,4},{6,7},{7,6},{8,9},{9,8},{10,11... | collective-permute-start | bytes 2457608 | tf_op jit(solution)/shard_map/ppermute | solution.py:54
  63.1 17.2 %collective-permute-start.6 = (bf16[8,32,2048]{2,1,0:T(8,128)(2,1)S(1)}, bf16[8,32,2048]{2,1,0:T(8,128)(2,1)}, u32[]{:S(2)}, u32[]{:S(2)}) collective-permute-start(bf16[8,32,2048]{2,1,0:T(8,128)(2,1)S(1)} %slice.45.refs_0_), channel_id=1, source_target_pairs={{0,8},{1,65},{2,10},{3,67},{4,12},{5,69},{6,14},{7,71},{8,16},{9,7... | collective-permute-start | bytes 3145736 | tf_op jit(solution)/shard_map/ppermute | solution.py:259
  67.5 1.1 copy-start.1
  72.2 10.2 %collective-permute-start.4 = (bf16[4,384,256]{2,1,0:T(8,128)(2,1)S(1)}, bf16[4,384,256]{2,1,0:T(8,128)(2,1)S(1)}, u32[]{:S(2)}, u32[]{:S(2)}) collective-permute-start(bf16[4,384,256]{2,1,0:T(8,128)(2,1)S(1)} %get-tuple-element.11), channel_id=1, source_target_pairs={{0,1},{1,0},{2,3},{3,2},{4,5},{5,4},{6,7},{7,6},{8,9},{9,8},{10,11... | collective-permute-start | bytes 2359304 | tf_op jit(solution)/shard_map/ppermute | solution.py:54
  74.2 15.9 %collective-permute-start.7 = (bf16[8,32,2048]{2,1,0:T(8,128)(2,1)S(1)}, bf16[8,32,2048]{2,1,0:T(8,128)(2,1)}, u32[]{:S(2)}, u32[]{:S(2)}) collective-permute-start(bf16[8,32,2048]{2,1,0:T(8,128)(2,1)S(1)} %slice.45.refs_0_), channel_id=1, source_target_pairs={{0,56},{1,449},{2,58},{3,451},{4,60},{5,453},{6,62},{7,455},{8,0},... | collective-permute-start | bytes 3145736 | tf_op jit(solution)/shard_map/ppermute | solution.py:262
  80.3 17.4 %collective-permute-start.8 = (bf16[8,32,2048]{2,1,0:T(8,128)(2,1)}, bf16[8,32,2048]{2,1,0:T(8,128)(2,1)}, u32[]{:S(2)}, u32[]{:S(2)}) collective-permute-start(bf16[8,32,2048]{2,1,0:T(8,128)(2,1)} %collective-permute-done.6.refs_1_), channel_id=1, source_target_pairs={{0,8},{1,65},{2,10},{3,67},{4,12},{5,69},{6,14},{7,71},{8,16},{9,7... | collective-permute-start | bytes 3145736 | tf_op jit(solution)/shard_map/ppermute | solution.py:259
  83.6 16.0 %all-to-all-start.2 = ((bf16[4,384,256]{2,1,0:T(8,128)(2,1)}), bf16[4,384,256]{2,1,0:T(8,128)(2,1)S(1)}, u32[]{:S(2)}, u32[]{:S(2)}) async-start(bf16[4,384,256]{2,1,0:T(8,128)(2,1)} %add_convert_fusion.1), calls=%async_computation.2 | async-start | bytes 1572864 | tf_op jit(solution)/shard_map/all_to_all | solution.py:77
  90.1 17.0 %collective-permute-start.9 = (bf16[8,32,2048]{2,1,0:T(8,128)(2,1)}, bf16[8,32,2048]{2,1,0:T(8,128)(2,1)}, u32[]{:S(2)}, u32[]{:S(2)}) collective-permute-start(bf16[8,32,2048]{2,1,0:T(8,128)(2,1)} %collective-permute-done.7.refs_2_), channel_id=1, source_target_pairs={{0,56},{1,449},{2,58},{3,451},{4,60},{5,453},{6,62},{7,455},{8,0},... | collective-permute-start | bytes 3145736 | tf_op jit(solution)/shard_map/ppermute | solution.py:262
  97.7 17.4 %collective-permute-start.10 = (bf16[8,32,2048]{2,1,0:T(8,128)(2,1)}, bf16[8,32,2048]{2,1,0:T(8,128)(2,1)}, u32[]{:S(2)}, u32[]{:S(2)}) collective-permute-start(bf16[8,32,2048]{2,1,0:T(8,128)(2,1)} %collective-permute-done.8.refs_3_), channel_id=1, source_target_pairs={{0,8},{1,65},{2,10},{3,67},{4,12},{5,69},{6,14},{7,71},{8,16},{9,7... | collective-permute-start | bytes 3145736 | tf_op jit(solution)/shard_map/ppermute | solution.py:259
  100.8 16.1 %all-to-all-start.3 = ((bf16[4,384,256]{2,1,0:T(8,128)(2,1)}), bf16[4,384,256]{2,1,0:T(8,128)(2,1)S(1)}, u32[]{:S(2)}, u32[]{:S(2)}) async-start(bf16[4,384,256]{2,1,0:T(8,128)(2,1)} %broadcast_in_dim.43), calls=%async_computation.3 | async-start | bytes 1572864 | tf_op jit(solution)/shard_map/all_to_all | solution.py:59
  107.1 17.4 %collective-permute-start.11 = (bf16[8,32,2048]{2,1,0:T(8,128)(2,1)}, bf16[8,32,2048]{2,1,0:T(8,128)(2,1)}, u32[]{:S(2)}, u32[]{:S(2)}) collective-permute-start(bf16[8,32,2048]{2,1,0:T(8,128)(2,1)} %collective-permute-done.9.refs_4_), channel_id=1, source_target_pairs={{0,56},{1,449},{2,58},{3,451},{4,60},{5,453},{6,62},{7,455},{8,0},... | collective-permute-start | bytes 3145736 | tf_op jit(solution)/shard_map/ppermute | solution.py:262
  115.0 17.4 %collective-permute-start.12 = (bf16[8,32,2048]{2,1,0:T(8,128)(2,1)}, bf16[8,32,2048]{2,1,0:T(8,128)(2,1)}, u32[]{:S(2)}, u32[]{:S(2)}) collective-permute-start(bf16[8,32,2048]{2,1,0:T(8,128)(2,1)} %collective-permute-done.10.refs_5_), channel_id=1, source_target_pairs={{0,8},{1,65},{2,10},{3,67},{4,12},{5,69},{6,14},{7,71},{8,16},{9,7... | collective-permute-start | bytes 3145736 | tf_op jit(solution)/shard_map/ppermute | solution.py:259
  116.9 15.4 %collective-permute-start.5 = (bf16[4,384,256]{2,1,0:T(8,128)(2,1)S(1)}, bf16[4,384,256]{2,1,0:T(8,128)(2,1)S(1)}, u32[]{:S(2)}, u32[]{:S(2)}) collective-permute-start(bf16[4,384,256]{2,1,0:T(8,128)(2,1)S(1)} %all-to-all-done.3.mix_ref), channel_id=1, source_target_pairs={{0,1},{1,0},{2,3},{3,2},{4,5},{5,4},{6,7},{7,6},{8,9},{9,8},{10,11... | collective-permute-start | bytes 2359304 | tf_op jit(solution)/shard_map/ppermute | solution.py:54
  132.4 1.1 copy-start.2
  143.6 7.2 %collective-permute-start.13 = (bf16[4,384,256]{2,1,0:T(8,128)(2,1)S(1)}, bf16[4,384,256]{2,1,0:T(8,128)(2,1)S(1)}, u32[]{:S(2)}, u32[]{:S(2)}) collective-permute-start(bf16[4,384,256]{2,1,0:T(8,128)(2,1)S(1)} %get-tuple-element.14), channel_id=1, source_target_pairs={{0,1},{1,0},{2,3},{3,2},{4,5},{5,4},{6,7},{7,6},{8,9},{9,8},{10,11... | collective-permute-start | bytes 2359304 | tf_op jit(solution)/shard_map/ppermute | solution.py:54
  165.5 8.9 %copy-start.6 = (f32[256]{0:T(256)S(1)}, f32[256]{0:T(256)}, u32[]{:S(2)}) copy-start(f32[256]{0:T(256)} %param.17) | copy-start | bytes 3076
  (2 other events, 2.0 us)

commit v3 on v2

--- a/solution.py
+++ b/solution.py
@@ -15,7 +15,7 @@
 EVERY = FS + TP
 bf16 = jnp.bfloat16
 f32 = jnp.float32
-OFFSETS = (0, 1, -1, 2, -2, 3, -3, 4)
+OFFSETS = (0, 1, -1, 2, -2, 3, -3, 4, 4)
 MEBI = 1024 * 1024
 
 
@@ -156,18 +156,23 @@
 
 
 def ff_kernel(rows, mine_ref, other_ref, mix_ref, mix_other_ref, *refs):
-    chunks, (keep_ref, send_ref, own_ref, mid_ref, hid_ref, w_ref, sems) = refs[:8], refs[8:]
+    chunks, (keep_ref, send_ref, own_ref, mid_ref, hid_ref, w_ref, sems) = refs[:9], refs[9:]
     x, core = lax.axis_index("x"), lax.axis_index("core")
     place = jnp.where(core == 0, lax.axis_index("y"), lax.axis_index("z"))
-    copies = []
-    for k, (chunk, offset) in enumerate(zip(chunks, OFFSETS)):
-        source = lax.rem(place + (8 - offset), 8)
-        for j in range(8):
-            copy = pltpu.make_async_copy(
-                chunk.at[j], w_ref.at[row_at(core, source, j)], sems.at[k, j]
-            )
-            copy.start()
-            copies.append(copy)
+    copies = [[], []]
+    for half in range(2):
+        where = pl.ds(half * 1024, 1024)
+        for k, (chunk, offset) in enumerate(zip(chunks, OFFSETS)):
+            source = lax.rem(place + (8 - offset), 8)
+            for i in range(8 if k < 7 else 4):
+                j = i + 4 if k == 8 else i
+                copy = pltpu.make_async_copy(
+                    chunk.at[i, :, where],
+                    w_ref.at[row_at(core, source, j), where],
+                    sems.at[half, min(k, 7), j],
+                )
+                copy.start()
+                copies[half].append(copy)
     step = rows // 3
     for t in range(3):
         part = pl.ds(t * step, step)
@@ -187,13 +192,15 @@
             gain = gain_of(tok, lax.rem(x + (4 - xb), 4), rows, 3)
             mid_ref[part, columns_of(xb, c)] = ((load() - mean) * inverse * gain).astype(bf16)
     own_ref[...] = mid_ref[:, columns_of(x, core)]
-    for copy in copies:
+    for copy in copies[0]:
         copy.wait()
     for n in range(4):
         where = slice(n * 256, (n + 1) * 256)
         up = jnp.dot(mid_ref[...], w_ref[:, where], preferred_element_type=f32)
         up = jnp.maximum(up, 0.0)
         hid_ref[:, where] = (up * up).astype(bf16)
+    for copy in copies[1]:
+        copy.wait()
     for xb in range(4):
         for ref, c in ((keep_ref, core), (send_ref, 1 - core)):
             term = lax.dot_general(
@@ -231,13 +238,13 @@
     return pl.pallas_call(
         functools.partial(ff_kernel, rows),
         out_shape=(block, block, jax.ShapeDtypeStruct((rows, width), bf16)),
-        in_specs=vmem(4) + [pl.BlockSpec(memory_space=pl.ANY)] * 8,
+        in_specs=vmem(4) + [pl.BlockSpec(memory_space=pl.ANY)] * 9,
         out_specs=tuple(vmem(3)),
         scratch_shapes=[
             pltpu.VMEM((rows, 8 * width), bf16),
             pltpu.VMEM((rows, 1024), bf16),
             pltpu.VMEM((2048, 2048), bf16),
-            pltpu.SemaphoreType.DMA((8, 8)),
+            pltpu.SemaphoreType.DMA((2, 8, 8)),
         ],
         compiler_params=pltpu.CompilerParams(vmem_limit_bytes=30 * MEBI),
         cost_estimate=pl.CostEstimate(flops=8_000_000_000, bytes_accessed=12_000_000, transcendentals=0),
@@ -256,11 +263,11 @@
     chunks = [chunk]
     up, down = chunk, chunk
     for hop in range(4):
+        if hop == 3:
+            up, down = up[:4], down[4:]
         up = lax.ppermute(up, EVERY, around(1))
-        chunks.append(up)
-        if hop < 3:
-            down = lax.ppermute(down, EVERY, around(-1))
-            chunks.append(down)
+        down = lax.ppermute(down, EVERY, around(-1))
+        chunks += [up, down]
     extended = jnp.concatenate(
         [tokens, in_three(gain_mixer), in_three(gain_mid), jnp.zeros((10, width), bf16)]
     )

time: 176 us -> 177 us (level)
  blocking collectives: 49.6 us -> 62.1 us
  waiting for transfers between devices: 34.1 us -> 26 us
  Pallas kernels: 13.7 us -> 11.8 us
  starting transfers between devices: 65.5 us -> 63.7 us
    all_to_all x1 -> x2, blocking collectives: 8.4 us -> 20.7 us  [everyone(): lax.all_to_all(jnp.broadcast_to(array[None], (count, *array.shape)), axis...]
    ppermute x4, waiting for transfers between devices: 15.6 us -> 6.16 us  [layer(): up = lax.ppermute(up, EVERY, around(1))]
    ppermute x3 -> x4, starting transfers between devices: 13.9 us -> 18.5 us  [layer(): down = lax.ppermute(down, EVERY, around(-1))]
    all_to_all x1 -> x0, starting transfers between devices: 3.49 us -> none  [everyone(): lax.all_to_all(jnp.broadcast_to(array[None], (count, *array.shape)), axis...]
    ppermute x4, starting transfers between devices: 16.2 us -> 14 us  [from_other_core(): return lax.ppermute(array, 'core', [(0, 1), (1, 0)])]
    pallas_call x1, Pallas kernels: 10.1 us -> 8.2 us  [feed_forward(): pl.pallas_call(functools.partial(ff_kernel, rows), out_shape=(block, bloc...]
    ppermute x3 -> x4, waiting for transfers between devices: 8.83 us -> 10 us  [layer(): down = lax.ppermute(down, EVERY, around(-1))]
  transfers between devices with their start and end apart: 17 -> 17, of which waited for: 10 -> 7; matrix products, arithmetic and copies ran while one was open for 2% -> 3% of each run, Pallas kernels for 2% -> 2%
where the time goes in v3:
time: 177 us; the launch traced here: 176 us
  starting transfers between devices  63.7 us (36%)
  blocking collectives  62.1 us (35%)
  waiting for transfers between devices  26 us (15%)
  Pallas kernels  11.8 us (7%)
  local copies, waits for them, and re-layouts  7.01 us (4%)
  other arithmetic  5.09 us (3%)
    all_to_all x1, blocking collectives, among(): lax.all_to_all(jnp.broadcast_to(array[None], (8, *array.shape)), EVERY, 0...  26.9 us
    all_to_all x2, blocking collectives, everyone(): lax.all_to_all(jnp.broadcast_to(array[None], (count, *array.shape)), axis...  20.7 us
    ppermute x4, starting transfers between devices, layer(): down = lax.ppermute(down, EVERY, around(-1))  18.5 us
    all_to_all x1, blocking collectives, scatter_sum_tp(): four = lax.all_to_all(chip, 'x', 0, 0, tiled=True).astype(f32)  14.5 us
    ppermute x4, starting transfers between devices, from_other_core(): return lax.ppermute(array, 'core', [(0, 1), (1, 0)])  14 us
    ppermute x4, waiting for transfers between devices, layer(): down = lax.ppermute(down, EVERY, around(-1))  10 us
    all_to_all x1, starting transfers between devices, among(): lax.all_to_all(jnp.broadcast_to(array[None], (8, *array.shape)), EVERY, 0...  9.74 us
    ppermute x3, starting transfers between devices, along_x(): return lax.ppermute(array, EVERY, pairs)  9.33 us
  transfers between devices with their start and end apart: 17, of which 7 were waited for; matrix products, arithmetic and copies ran while one was open for 3% of the time, Pallas kernels for 2%

profile of v3, /device:TPU:1, one launch (start us, length us, event | category | flops | bytes accessed | tf_op | source)
XLA Modules:
  0.0 176.2 jit_solution(10010330800596637817)
XLA Ops:
  1.0 26.9 %all_to_all.30 = bf16[8,32,2304]{2,1,0:T(8,128)(2,1)S(1)} all-to-all(bf16[8,32,2304]{2,1,0:T(8,128)(2,1)S(1)} %broadcast_in_dim.17), channel_id=1, replica_groups={{0,64,128,192,256,320,384,448},{2,66,130,194,258,322,386,450},{4,68,132..., dimensions={0} | all-to-all | bytes 2359296 | tf_op jit(solution)/shard_map/all_to_all | solution.py:65
  30.0 9.7 %all-to-all-start.1 = ((bf16[8,256,256]{2,1,0:T(8,128)(2,1)}), bf16[8,256,256]{2,1,0:T(8,128)(2,1)S(1)}, u32[]{:S(2)}, u32[]{:S(2)}) async-start(bf16[8,256,256]{2,1,0:T(8,128)(2,1)} %broadcast_in_dim.19), calls=%async_computation.1 | async-start | bytes 2097152 | tf_op jit(solution)/shard_map/all_to_all | solution.py:65
  40.2 4.4 %collective-permute-start.2 = (bf16[400,256]{1,0:T(8,128)(2,1)S(1)}, bf16[400,256]{1,0:T(8,128)(2,1)S(1)}, u32[]{:S(2)}, u32[]{:S(2)}) collective-permute-start(bf16[400,256]{1,0:T(8,128)(2,1)S(1)} %concatenate.10), channel_id=1, source_target_pairs={{0,6},{1,7},{2,0},{3,1},{4,2},{5,3},{6,4},{7,5},{8,14},{9,15},{10,... | collective-permute-start | bytes 614408 | tf_op jit(solution)/shard_map/ppermute | solution.py:50
  44.6 2.4 %collective-permute-start.1 = (bf16[400,256]{1,0:T(8,128)(2,1)S(1)}, bf16[400,256]{1,0:T(8,128)(2,1)S(1)}, u32[]{:S(2)}, u32[]{:S(2)}) collective-permute-start(bf16[400,256]{1,0:T(8,128)(2,1)S(1)} %concatenate.10), channel_id=1, source_target_pairs={{0,4},{1,5},{2,6},{3,7},{4,0},{5,1},{6,2},{7,3},{8,12},{9,13},{10,... | collective-permute-start | bytes 614408 | tf_op jit(solution)/shard_map/ppermute | solution.py:50
  47.0 2.5 %collective-permute-start = (bf16[400,256]{1,0:T(8,128)(2,1)S(1)}, bf16[400,256]{1,0:T(8,128)(2,1)S(1)}, u32[]{:S(2)}, u32[]{:S(2)}) collective-permute-start(bf16[400,256]{1,0:T(8,128)(2,1)S(1)} %concatenate.10), channel_id=1, source_target_pairs={{0,2},{1,3},{2,4},{3,5},{4,6},{5,7},{6,0},{7,1},{8,10},{9,11},{10,... | collective-permute-start | bytes 614408 | tf_op jit(solution)/shard_map/ppermute | solution.py:50
  49.5 3.3 %collective-permute-done.1 = bf16[400,256]{1,0:T(8,128)(2,1)S(1)} collective-permute-done((bf16[400,256]{1,0:T(8,128)(2,1)S(1)}, bf16[400,256]{1,0:T(8,128)(2,1)S(1)}, u32[]{:S(2)}, u32[]{:S(2)}) %collective-permute-start.1) | collective-permute-done | bytes 204832 | tf_op jit(solution)/shard_map/ppermute | solution.py:50
  52.9 4.4 %collective-permute-done = bf16[400,256]{1,0:T(8,128)(2,1)S(1)} collective-permute-done((bf16[400,256]{1,0:T(8,128)(2,1)S(1)}, bf16[400,256]{1,0:T(8,128)(2,1)S(1)}, u32[]{:S(2)}, u32[]{:S(2)}) %collective-permute-start) | collective-permute-done | bytes 204832 | tf_op jit(solution)/shard_map/ppermute | solution.py:50
  57.4 4.4 %collective-permute-start.3 = (bf16[4,400,256]{2,1,0:T(8,128)(2,1)S(1)}, bf16[4,400,256]{2,1,0:T(8,128)(2,1)S(1)}, u32[]{:S(2)}, u32[]{:S(2)}) collective-permute-start(bf16[4,400,256]{2,1,0:T(8,128)(2,1)S(1)} %pad_maximum_fusion.mine_ref), channel_id=1, source_target_pairs={{0,1},{1,0},{2,3},{3,2},{4,5},{5,4},{6,7},{7,6},{8,9},{9,8},{10,11... | collective-permute-start | bytes 2457608 | tf_op jit(solution)/shard_map/ppermute | solution.py:54
  63.2 3.7 %collective-permute-start.7 = (bf16[8,32,2048]{2,1,0:T(8,128)(2,1)S(1)}, bf16[8,32,2048]{2,1,0:T(8,128)(2,1)}, u32[]{:S(2)}, u32[]{:S(2)}) collective-permute-start(bf16[8,32,2048]{2,1,0:T(8,128)(2,1)S(1)} %slice.53.refs_0_), channel_id=1, source_target_pairs={{0,56},{1,449},{2,58},{3,451},{4,60},{5,453},{6,62},{7,455},{8,0},... | collective-permute-start | bytes 3145736 | tf_op jit(solution)/shard_map/ppermute | solution.py:269
  70.9 3.6 %mixer.1 = (bf16[4,384,256]{2,1,0:T(8,128)(2,1)S(1)}, bf16[4,384,256]{2,1,0:T(8,128)(2,1)S(1)}) custom-call(bf16[4,400,256]{2,1,0:T(8,128)(2,1)S(1)} %pad_maximum_fusion.mine_ref, bf16[4,400,256]{2,1,0:T(8,128)(2,1)S(1)} %copy-done.1, bf16[8,8,32,256]{3,2,1,0:T(8,128)(2,1)S(1)} %bitcast.16, f32[1,128]{1,0:T(1,128)S(1)} %bitcast.17), custom_call_target="tpu_custom_call" | custom-call | flops 4000000000 | bytes 4000000 | tf_op jit(solution)/shard_map/mixer/pallas_call | solution.py:221
  74.5 2.3 %collective-permute-start.4 = (bf16[4,384,256]{2,1,0:T(8,128)(2,1)S(1)}, bf16[4,384,256]{2,1,0:T(8,128)(2,1)S(1)}, u32[]{:S(2)}, u32[]{:S(2)}) collective-permute-start(bf16[4,384,256]{2,1,0:T(8,128)(2,1)S(1)} %get-tuple-element.11), channel_id=1, source_target_pairs={{0,1},{1,0},{2,3},{3,2},{4,5},{5,4},{6,7},{7,6},{8,9},{9,8},{10,11... | collective-permute-start | bytes 2359304 | tf_op jit(solution)/shard_map/ppermute | solution.py:54
  76.8 2.3 %collective-permute-done.7.refs_2_ = bf16[8,32,2048]{2,1,0:T(8,128)(2,1)} collective-permute-done((bf16[8,32,2048]{2,1,0:T(8,128)(2,1)S(1)}, bf16[8,32,2048]{2,1,0:T(8,128)(2,1)}, u32[]{:S(2)}, u32[]{:S(2)}) %collective-permute-start.7) | collective-permute-done | bytes 1048608 | tf_op jit(solution)/shard_map/ppermute | solution.py:269
  79.1 4.9 %collective-permute-start.9 = (bf16[8,32,2048]{2,1,0:T(8,128)(2,1)}, bf16[8,32,2048]{2,1,0:T(8,128)(2,1)}, u32[]{:S(2)}, u32[]{:S(2)}) collective-permute-start(bf16[8,32,2048]{2,1,0:T(8,128)(2,1)} %collective-permute-done.7.refs_2_), channel_id=1, source_target_pairs={{0,56},{1,449},{2,58},{3,451},{4,60},{5,453},{6,62},{7,455},{8,0},... | collective-permute-start | bytes 3145736 | tf_op jit(solution)/shard_map/ppermute | solution.py:269
  87.0 4.2 %all-to-all-start.2 = ((bf16[4,384,256]{2,1,0:T(8,128)(2,1)}), bf16[4,384,256]{2,1,0:T(8,128)(2,1)}, u32[]{:S(2)}, u32[]{:S(2)}) async-start(bf16[4,384,256]{2,1,0:T(8,128)(2,1)} %add_convert_fusion.1), calls=%async_computation.2 | async-start | bytes 1572864 | tf_op jit(solution)/shard_map/all_to_all | solution.py:77
  91.2 4.8 %collective-permute-done.9.refs_4_ = bf16[8,32,2048]{2,1,0:T(8,128)(2,1)} collective-permute-done((bf16[8,32,2048]{2,1,0:T(8,128)(2,1)}, bf16[8,32,2048]{2,1,0:T(8,128)(2,1)}, u32[]{:S(2)}, u32[]{:S(2)}) %collective-permute-start.9) | collective-permute-done | bytes 1048608 | tf_op jit(solution)/shard_map/ppermute | solution.py:269
  96.0 5.3 %collective-permute-start.11 = (bf16[8,32,2048]{2,1,0:T(8,128)(2,1)}, bf16[8,32,2048]{2,1,0:T(8,128)(2,1)S(1)}, u32[]{:S(2)}, u32[]{:S(2)}) collective-permute-start(bf16[8,32,2048]{2,1,0:T(8,128)(2,1)} %collective-permute-done.9.refs_4_), channel_id=1, source_target_pairs={{0,56},{1,449},{2,58},{3,451},{4,60},{5,453},{6,62},{7,455},{8,0},... | collective-permute-start | bytes 3145736 | tf_op jit(solution)/shard_map/ppermute | solution.py:269
  104.7 12.5 %all_to_all.31.mix_ref = bf16[4,384,256]{2,1,0:T(8,128)(2,1)S(1)} all-to-all(bf16[4,384,256]{2,1,0:T(8,128)(2,1)S(1)} %broadcast_in_dim.43), channel_id=1, replica_groups=mesh['z'=8,'y'=8,'x'=4,'core'=2] {'x'}, dimensions={0} | all-to-all | bytes 1572864 | tf_op jit(solution)/shard_map/all_to_all | solution.py:59
  117.3 5.1 %collective-permute-start.5 = (bf16[4,384,256]{2,1,0:T(8,128)(2,1)S(1)}, bf16[4,384,256]{2,1,0:T(8,128)(2,1)S(1)}, u32[]{:S(2)}, u32[]{:S(2)}) collective-permute-start(bf16[4,384,256]{2,1,0:T(8,128)(2,1)S(1)} %all_to_all.31.mix_ref), channel_id=1, source_target_pairs={{0,1},{1,0},{2,3},{3,2},{4,5},{5,4},{6,7},{7,6},{8,9},{9,8},{10,11... | collective-permute-start | bytes 2359304 | tf_op jit(solution)/shard_map/ppermute | solution.py:54
  122.5 4.7 %collective-permute-start.13 = (bf16[4,32,2048]{2,1,0:T(8,128)(2,1)S(1)}, bf16[4,32,2048]{2,1,0:T(8,128)(2,1)S(1)}, u32[]{:S(2)}, u32[]{:S(2)}) collective-permute-start(bf16[4,32,2048]{2,1,0:T(8,128)(2,1)S(1)} %slice.55), channel_id=1, source_target_pairs={{0,56},{1,449},{2,58},{3,451},{4,60},{5,453},{6,62},{7,455},{8,0},... | collective-permute-start | bytes 1572872 | tf_op jit(solution)/shard_map/ppermute | solution.py:269
  130.3 2.9 %collective-permute-done.13.refs_8_ = bf16[4,32,2048]{2,1,0:T(8,128)(2,1)S(1)} collective-permute-done((bf16[4,32,2048]{2,1,0:T(8,128)(2,1)S(1)}, bf16[4,32,2048]{2,1,0:T(8,128)(2,1)S(1)}, u32[]{:S(2)}, u32[]{:S(2)}) %collective-permute-start.13) | collective-permute-done | bytes 524320 | tf_op jit(solution)/shard_map/ppermute | solution.py:269
  133.2 6.1 %collective-permute-done.12.refs_7_ = bf16[4,32,2048]{2,1,0:T(8,128)(2,1)S(1)} collective-permute-done((bf16[4,32,2048]{2,1,0:T(8,128)(2,1)S(1)}, bf16[4,32,2048]{2,1,0:T(8,128)(2,1)S(1)}, u32[]{:S(2)}, u32[]{:S(2)}) %collective-permute-start.12) | collective-permute-done | bytes 524320 | tf_op jit(solution)/shard_map/ppermute | solution.py:268
  139.4 8.2 %feed_forward.1 = (bf16[4,384,256]{2,1,0:T(8,128)(2,1)S(1)}, bf16[4,384,256]{2,1,0:T(8,128)(2,1)S(1)}, bf16[384,256]{1,0:T(8,128)(2,1)S(1)}) custom-call(bf16[4,400,256]{2,1,0:T(8,128)(2,1)S(1)} %pad_maximum_fusion.mine_ref, bf16[4,400,256]{2,1,0:T(8,128)(2,1)S(1)} %copy-done.2, bf16[4,384,256]{2,1,0:T(8,128)(2,1)S(1)} %all_to_all.31.mix_ref, ...), custom_call_target="tpu_custom_call" | custom-call | flops 8000000000 | bytes 12000000 | tf_op jit(solution)/shard_map/feed_forward/pallas_call | solution.py:238
  152.0 14.5 %all_to_all.32 = bf16[4,384,256]{2,1,0:T(8,128)(2,1)S(1)} all-to-all(bf16[4,384,256]{2,1,0:T(8,128)(2,1)S(1)} %add_convert_fusion), channel_id=1, replica_groups=mesh['z'=8,'y'=8,'x'=4,'core'=2] {'x'}, dimensions={0} | all-to-all | bytes 1572864 | tf_op jit(solution)/shard_map/all_to_all | solution.py:77
  167.1 8.2 %all_to_all.33 = f32[8,1,768]{2,1,0:T(1,128)S(1)} all-to-all(f32[8,1,768]{2,1,0:T(1,128)S(1)} %broadcast_in_dim.44), channel_id=1, replica_groups=mesh['z'=8,'y'=8,'x'=4,'core'=2] {'x','core'}, dimensions={0} | all-to-all | bytes 49152 | tf_op jit(solution)/shard_map/all_to_all | solution.py:59
  (69 shorter events, 24.2 us)
Async XLA Ops:
  29.0 10.8 %copy-start.7 = (f32[256]{0:T(256)S(1)}, f32[256]{0:T(256)}, u32[]{:S(2)}) copy-start(f32[256]{0:T(256)} %param.10) | copy-start | bytes 3076
  29.0 10.9 %copy-start.8 = (f32[256]{0:T(256)S(1)}, f32[256]{0:T(256)}, u32[]{:S(2)}) copy-start(f32[256]{0:T(256)} %param.14) | copy-start | bytes 3076
  29.0 10.9 %copy-start.5 = (bf16[384,256]{1,0:T(8,128)(2,1)S(1)}, bf16[384,256]{1,0:T(8,128)(2,1)}, u32[]{:S(2)}) copy-start(bf16[384,256]{1,0:T(8,128)(2,1)} %param.9) | copy-start | bytes 589828
  30.0 39.7 %all-to-all-start.1 = ((bf16[8,256,256]{2,1,0:T(8,128)(2,1)}), bf16[8,256,256]{2,1,0:T(8,128)(2,1)S(1)}, u32[]{:S(2)}, u32[]{:S(2)}) async-start(bf16[8,256,256]{2,1,0:T(8,128)(2,1)} %broadcast_in_dim.19), calls=%async_computation.1 | async-start | bytes 2097152 | tf_op jit(solution)/shard_map/all_to_all | solution.py:65
  40.2 9.4 %collective-permute-start.2 = (bf16[400,256]{1,0:T(8,128)(2,1)S(1)}, bf16[400,256]{1,0:T(8,128)(2,1)S(1)}, u32[]{:S(2)}, u32[]{:S(2)}) collective-permute-start(bf16[400,256]{1,0:T(8,128)(2,1)S(1)} %concatenate.10), channel_id=1, source_target_pairs={{0,6},{1,7},{2,0},{3,1},{4,2},{5,3},{6,4},{7,5},{8,14},{9,15},{10,... | collective-permute-start | bytes 614408 | tf_op jit(solution)/shard_map/ppermute | solution.py:50
  44.6 8.3 %collective-permute-start.1 = (bf16[400,256]{1,0:T(8,128)(2,1)S(1)}, bf16[400,256]{1,0:T(8,128)(2,1)S(1)}, u32[]{:S(2)}, u32[]{:S(2)}) collective-permute-start(bf16[400,256]{1,0:T(8,128)(2,1)S(1)} %concatenate.10), channel_id=1, source_target_pairs={{0,4},{1,5},{2,6},{3,7},{4,0},{5,1},{6,2},{7,3},{8,12},{9,13},{10,... | collective-permute-start | bytes 614408 | tf_op jit(solution)/shard_map/ppermute | solution.py:50
  47.0 10.3 %collective-permute-start = (bf16[400,256]{1,0:T(8,128)(2,1)S(1)}, bf16[400,256]{1,0:T(8,128)(2,1)S(1)}, u32[]{:S(2)}, u32[]{:S(2)}) collective-permute-start(bf16[400,256]{1,0:T(8,128)(2,1)S(1)} %concatenate.10), channel_id=1, source_target_pairs={{0,2},{1,3},{2,4},{3,5},{4,6},{5,7},{6,0},{7,1},{8,10},{9,11},{10,... | collective-permute-start | bytes 614408 | tf_op jit(solution)/shard_map/ppermute | solution.py:50
  57.3 12.4 %copy-start.3 = (f32[128]{0:T(128)S(1)}, f32[128]{0:T(128)}, u32[]{:S(2)}) copy-start(f32[128]{0:T(128)} %param.12) | copy-start | bytes 1540
  57.4 11.4 %collective-permute-start.3 = (bf16[4,400,256]{2,1,0:T(8,128)(2,1)S(1)}, bf16[4,400,256]{2,1,0:T(8,128)(2,1)S(1)}, u32[]{:S(2)}, u32[]{:S(2)}) collective-permute-start(bf16[4,400,256]{2,1,0:T(8,128)(2,1)S(1)} %pad_maximum_fusion.mine_ref), channel_id=1, source_target_pairs={{0,1},{1,0},{2,3},{3,2},{4,5},{5,4},{6,7},{7,6},{8,9},{9,8},{10,11... | collective-permute-start | bytes 2457608 | tf_op jit(solution)/shard_map/ppermute | solution.py:54
  63.2 15.9 %collective-permute-start.7 = (bf16[8,32,2048]{2,1,0:T(8,128)(2,1)S(1)}, bf16[8,32,2048]{2,1,0:T(8,128)(2,1)}, u32[]{:S(2)}, u32[]{:S(2)}) collective-permute-start(bf16[8,32,2048]{2,1,0:T(8,128)(2,1)S(1)} %slice.53.refs_0_), channel_id=1, source_target_pairs={{0,56},{1,449},{2,58},{3,451},{4,60},{5,453},{6,62},{7,455},{8,0},... | collective-permute-start | bytes 3145736 | tf_op jit(solution)/shard_map/ppermute | solution.py:269
  66.9 17.2 %collective-permute-start.6 = (bf16[8,32,2048]{2,1,0:T(8,128)(2,1)S(1)}, bf16[8,32,2048]{2,1,0:T(8,128)(2,1)}, u32[]{:S(2)}, u32[]{:S(2)}) collective-permute-start(bf16[8,32,2048]{2,1,0:T(8,128)(2,1)S(1)} %slice.53.refs_0_), channel_id=1, source_target_pairs={{0,8},{1,65},{2,10},{3,67},{4,12},{5,69},{6,14},{7,71},{8,16},{9,7... | collective-permute-start | bytes 3145736 | tf_op jit(solution)/shard_map/ppermute | solution.py:268
  69.7 1.1 copy-start.1
  74.5 11.5 %collective-permute-start.4 = (bf16[4,384,256]{2,1,0:T(8,128)(2,1)S(1)}, bf16[4,384,256]{2,1,0:T(8,128)(2,1)S(1)}, u32[]{:S(2)}, u32[]{:S(2)}) collective-permute-start(bf16[4,384,256]{2,1,0:T(8,128)(2,1)S(1)} %get-tuple-element.11), channel_id=1, source_target_pairs={{0,1},{1,0},{2,3},{3,2},{4,5},{5,4},{6,7},{7,6},{8,9},{9,8},{10,11... | collective-permute-start | bytes 2359304 | tf_op jit(solution)/shard_map/ppermute | solution.py:54
  79.1 16.9 %collective-permute-start.9 = (bf16[8,32,2048]{2,1,0:T(8,128)(2,1)}, bf16[8,32,2048]{2,1,0:T(8,128)(2,1)}, u32[]{:S(2)}, u32[]{:S(2)}) collective-permute-start(bf16[8,32,2048]{2,1,0:T(8,128)(2,1)} %collective-permute-done.7.refs_2_), channel_id=1, source_target_pairs={{0,56},{1,449},{2,58},{3,451},{4,60},{5,453},{6,62},{7,455},{8,0},... | collective-permute-start | bytes 3145736 | tf_op jit(solution)/shard_map/ppermute | solution.py:269
  84.0 17.4 %collective-permute-start.8 = (bf16[8,32,2048]{2,1,0:T(8,128)(2,1)}, bf16[8,32,2048]{2,1,0:T(8,128)(2,1)}, u32[]{:S(2)}, u32[]{:S(2)}) collective-permute-start(bf16[8,32,2048]{2,1,0:T(8,128)(2,1)} %collective-permute-done.6.refs_1_), channel_id=1, source_target_pairs={{0,8},{1,65},{2,10},{3,67},{4,12},{5,69},{6,14},{7,71},{8,16},{9,7... | collective-permute-start | bytes 3145736 | tf_op jit(solution)/shard_map/ppermute | solution.py:268
  87.0 16.3 %all-to-all-start.2 = ((bf16[4,384,256]{2,1,0:T(8,128)(2,1)}), bf16[4,384,256]{2,1,0:T(8,128)(2,1)}, u32[]{:S(2)}, u32[]{:S(2)}) async-start(bf16[4,384,256]{2,1,0:T(8,128)(2,1)} %add_convert_fusion.1), calls=%async_computation.2 | async-start | bytes 1572864 | tf_op jit(solution)/shard_map/all_to_all | solution.py:77
  96.0 26.4 %collective-permute-start.11 = (bf16[8,32,2048]{2,1,0:T(8,128)(2,1)}, bf16[8,32,2048]{2,1,0:T(8,128)(2,1)S(1)}, u32[]{:S(2)}, u32[]{:S(2)}) collective-permute-start(bf16[8,32,2048]{2,1,0:T(8,128)(2,1)} %collective-permute-done.9.refs_4_), channel_id=1, source_target_pairs={{0,56},{1,449},{2,58},{3,451},{4,60},{5,453},{6,62},{7,455},{8,0},... | collective-permute-start | bytes 3145736 | tf_op jit(solution)/shard_map/ppermute | solution.py:269
  101.4 25.8 %collective-permute-start.10 = (bf16[8,32,2048]{2,1,0:T(8,128)(2,1)}, bf16[8,32,2048]{2,1,0:T(8,128)(2,1)}, u32[]{:S(2)}, u32[]{:S(2)}) collective-permute-start(bf16[8,32,2048]{2,1,0:T(8,128)(2,1)} %collective-permute-done.8.refs_3_), channel_id=1, source_target_pairs={{0,8},{1,65},{2,10},{3,67},{4,12},{5,69},{6,14},{7,71},{8,16},{9,7... | collective-permute-start | bytes 3145736 | tf_op jit(solution)/shard_map/ppermute | solution.py:268
  104.7 34.7 %copy-start.2 = (bf16[4,400,256]{2,1,0:T(8,128)(2,1)S(1)}, bf16[4,400,256]{2,1,0:T(8,128)(2,1)}, u32[]{:S(2)}) copy-start(bf16[4,400,256]{2,1,0:T(8,128)(2,1)} %copy-done) | copy-start | bytes 2457604
  117.3 22.1 %collective-permute-start.5 = (bf16[4,384,256]{2,1,0:T(8,128)(2,1)S(1)}, bf16[4,384,256]{2,1,0:T(8,128)(2,1)S(1)}, u32[]{:S(2)}, u32[]{:S(2)}) collective-permute-start(bf16[4,384,256]{2,1,0:T(8,128)(2,1)S(1)} %all_to_all.31.mix_ref), channel_id=1, source_target_pairs={{0,1},{1,0},{2,3},{3,2},{4,5},{5,4},{6,7},{7,6},{8,9},{9,8},{10,11... | collective-permute-start | bytes 2359304 | tf_op jit(solution)/shard_map/ppermute | solution.py:54
  122.5 10.8 %collective-permute-start.13 = (bf16[4,32,2048]{2,1,0:T(8,128)(2,1)S(1)}, bf16[4,32,2048]{2,1,0:T(8,128)(2,1)S(1)}, u32[]{:S(2)}, u32[]{:S(2)}) collective-permute-start(bf16[4,32,2048]{2,1,0:T(8,128)(2,1)S(1)} %slice.55), channel_id=1, source_target_pairs={{0,56},{1,449},{2,58},{3,451},{4,60},{5,453},{6,62},{7,455},{8,0},... | collective-permute-start | bytes 1572872 | tf_op jit(solution)/shard_map/ppermute | solution.py:269
  128.2 11.1 %collective-permute-start.12 = (bf16[4,32,2048]{2,1,0:T(8,128)(2,1)S(1)}, bf16[4,32,2048]{2,1,0:T(8,128)(2,1)S(1)}, u32[]{:S(2)}, u32[]{:S(2)}) collective-permute-start(bf16[4,32,2048]{2,1,0:T(8,128)(2,1)S(1)} %slice.54), channel_id=1, source_target_pairs={{0,8},{1,65},{2,10},{3,67},{4,12},{5,69},{6,14},{7,71},{8,16},{9,7... | collective-permute-start | bytes 1572872 | tf_op jit(solution)/shard_map/ppermute | solution.py:268
  147.6 4.2 %collective-permute-start.14 = (bf16[4,384,256]{2,1,0:T(8,128)(2,1)S(1)}, bf16[4,384,256]{2,1,0:T(8,128)(2,1)S(1)}, u32[]{:S(2)}, u32[]{:S(2)}) collective-permute-start(bf16[4,384,256]{2,1,0:T(8,128)(2,1)S(1)} %get-tuple-element.14), channel_id=1, source_target_pairs={{0,1},{1,0},{2,3},{3,2},{4,5},{5,4},{6,7},{7,6},{8,9},{9,8},{10,11... | collective-permute-start | bytes 2359304 | tf_op jit(solution)/shard_map/ppermute | solution.py:54
  166.6 8.7 %copy-start.6 = (f32[256]{0:T(256)S(1)}, f32[256]{0:T(256)}, u32[]{:S(2)}) copy-start(f32[256]{0:T(256)} %param.17) | copy-start | bytes 3076
  (2 other events, 2.0 us)
